TPU v7x, 32 devices: a whole 2x2x4 slice. The times are simulated.
32 devices in a mesh: grp: 1, ep: 32 (over z, y, x, core).
Axes of the slice: x: 2, y: 2, z: 4, core: 2. Of those that a mesh axis runs over, the one named last changes fastest.
Arguments:
- residual_input: bfloat16 [768, 2048], P(('grp', 'ep')), may hold values from -6 to 6
- attention_norm_gain: bfloat16 [2048], replicated, may hold values from 0.099609375 to 1.8984375
- receptance_weight: bfloat16 [2048, 1024], P(None, 'ep'), may hold values from -0.125 to 0.125
- key_weight: bfloat16 [2048, 1024], P(None, 'ep'), may hold values from -0.125 to 0.125
- value_weight: bfloat16 [2048, 1024], P(None, 'ep'), may hold values from -0.125 to 0.125
- decay_weight: bfloat16 [2048, 1024], P(None, 'ep'), may hold values from -0.125 to 0.125
- correction_rate_weight: bfloat16 [2048, 1024], P(None, 'ep'), may hold values from -0.125 to 0.125
- output_gate_weight: bfloat16 [2048, 1024], P(None, 'ep'), may hold values from -0.125 to 0.125
- decay_offset: float32 [1024], replicated, may hold values from -3 to 1
- correction_rate_offset: float32 [1024], replicated, may hold values from -1.5 to 1.5
- self_term_weight: float32 [1024], replicated, may hold values from -2 to 2
- head_read_gain: float32 [1024], replicated, may hold values from 0.1 to 1.9
- previous_state: float32 [768, 16, 4096], P(('grp', 'ep')), may hold values from -4 to 4
- attention_output_weight: bfloat16 [1024, 2048], replicated, may hold values from -0.1875 to 0.1875
- feedforward_norm_gain: bfloat16 [2048], replicated, may hold values from 0.099609375 to 1.8984375
- routes: int32 [768, 4], P('grp'), may hold values from 0 to 31, all different within a row; in each aligned block of 24 rows (0 to 23, 24 to 47, ...) at most 4 rows name the same one
- routing_weight: float32 [768, 4], P('grp'), may hold values from 0.2 to 1
- routed_gate_weight: bfloat16 [32, 2048, 512], P('ep'), may hold values from -0.125 to 0.125
- routed_up_weight: bfloat16 [32, 2048, 512], P('ep'), may hold values from -0.125 to 0.125
- routed_down_weight: bfloat16 [32, 512, 2048], P('ep'), may hold values from -0.25 to 0.25
- common_gate_weight: bfloat16 [2048, 512], replicated, may hold values from -0.125 to 0.125
- common_up_weight: bfloat16 [2048, 512], replicated, may hold values from -0.125 to 0.125
- common_down_weight: bfloat16 [512, 2048], replicated, may hold values from -0.25 to 0.25
Outputs:
- hidden_out: bfloat16 [768, 2048], P(('grp', 'ep'))
- next_state: float32 [768, 16, 4096], P(('grp', 'ep'))
Inputs may be any that keep to these rules, and one draw needn't show every extreme that they name: `routes`: the 4 entries of a row differ. In each aligned block of 24 rows (the tokens of one index of ep) no expert is named by more than 4 rows, a bound that some block reaches.
All inputs are finite; a program needn't handle non-finite values.
Results may differ from a plain program's by a relative error of at most 0.013.
Values may be sent and summed in bfloat16 or wider, within the bound.
A program may use at most 128 MiB of HBM per device.

v0:
```python
import jax
import jax.numpy as jnp
from jax import lax
from jax.sharding import PartitionSpec as P

HEAD_COUNT = 16
HEAD_SIZE = 64
CAP = 4


def rms_norm(value_rows, gain):
    scale = lax.rsqrt(jnp.mean(value_rows * value_rows, axis=-1, keepdims=True) + 1e-06)
    return (value_rows * scale * gain.astype(jnp.float32)).astype(jnp.bfloat16)


def expert_mlp(rows, gate_w, up_w, down_w):
    gate = jnp.dot(rows, gate_w, preferred_element_type=jnp.float32)
    upward = jnp.dot(rows, up_w, preferred_element_type=jnp.float32)
    hidden = (jax.nn.silu(gate) * upward).astype(jnp.bfloat16)
    return jnp.dot(hidden, down_w, preferred_element_type=jnp.float32).astype(jnp.bfloat16)


def attention_mixer(
    receptance_rows,
    key_rows,
    value_rows,
    decay_logit,
    rate_logit,
    gate_logit,
    decay_offset,
    correction_rate_offset,
    self_term_weight,
    head_read_gain,
    head_state,
):
    tally_value = receptance_rows.shape[0]

    def heads(tensor):
        return tensor.astype(jnp.float32).reshape(tally_value, HEAD_COUNT, HEAD_SIZE)

    decay = jnp.exp(
        -jnp.exp(-jax.nn.softplus(-(decay_offset + decay_logit.astype(jnp.float32))) - 0.5)
    )
    rate = jax.nn.sigmoid(correction_rate_offset + rate_logit.astype(jnp.float32))
    key_head = heads(key_rows)
    rate_head = heads(rate)
    receptance_head = heads(receptance_rows)
    head_value = heads(value_rows)
    unit_key = key_head * lax.rsqrt(1.0 + jnp.sum(key_head * key_head, axis=-1, keepdims=True))
    rate_scaled_key = key_head * rate_head
    removal = unit_key * rate_head
    matrix = head_state.reshape(tally_value, HEAD_COUNT, HEAD_SIZE, HEAD_SIZE)
    recalled = jnp.einsum("nhvk,nhk->nhv", matrix, unit_key, precision=lax.Precision.HIGHEST)
    matrix = (
        matrix * heads(decay)[:, :, None, :]
        - recalled[..., None] * removal[:, :, None, :]
        + head_value[..., None] * rate_scaled_key[:, :, None, :]
    )
    read = jnp.einsum("nhvk,nhk->nhv", matrix, receptance_head, precision=lax.Precision.HIGHEST)
    centered = read - jnp.mean(read, axis=-1, keepdims=True)
    variance = jnp.mean(centered * centered, axis=-1, keepdims=True)
    normed_head_read = (
        centered * lax.rsqrt(variance + 0.00064) * head_read_gain.reshape(HEAD_COUNT, HEAD_SIZE)
    )
    self_term = (
        jnp.sum(
            receptance_head * rate_scaled_key * self_term_weight.reshape(HEAD_COUNT, HEAD_SIZE),
            axis=-1,
            keepdims=True,
        )
        * head_value
    )
    normed_mixer_input = (normed_head_read + self_term).reshape(
        tally_value, HEAD_COUNT * HEAD_SIZE
    ) * jax.nn.sigmoid(gate_logit.astype(jnp.float32))
    return (
        normed_mixer_input.astype(jnp.bfloat16),
        matrix.reshape(tally_value, HEAD_COUNT, HEAD_SIZE * HEAD_SIZE),
    )


def slot_table(block_routes, block_weight, expert_ids):
    match = block_routes[..., None] == expert_ids
    hit = jnp.any(match, axis=-2).astype(jnp.int32)
    weight = jnp.sum(jnp.where(match, block_weight[..., None], 0.0), axis=-2)
    rank = jnp.cumsum(hit, axis=-2) - hit
    slots = jnp.arange(CAP, dtype=jnp.int32)
    select = ((hit[..., None] == 1) & (rank[..., None] == slots)).astype(jnp.float32)
    return (select, weight)


def combine_returned(select, weight, returned):
    coefficient = select * weight[..., None]
    return jnp.einsum(
        "nec,ecd->nd", coefficient, returned.astype(jnp.float32), precision=lax.Precision.HIGHEST
    )


def serve_gathered(
    whole, routes, routing_weight, ep_size, tally_value, expert_ids, gate_w, up_w, down_w
):
    block_routes = routes.reshape(ep_size, tally_value, routes.shape[-1])
    block_weight = routing_weight.reshape(ep_size, tally_value, routing_weight.shape[-1])
    select, weight = slot_table(block_routes, block_weight, expert_ids)
    select = select[:, :, 0, :]
    weight = weight[:, :, 0]
    rows = jnp.einsum(
        "snc,snd->scd",
        select.astype(jnp.bfloat16),
        whole.reshape(ep_size, tally_value, whole.shape[-1]),
        preferred_element_type=jnp.float32,
    ).astype(jnp.bfloat16)
    output = expert_mlp(rows.reshape(-1, rows.shape[-1]), gate_w, up_w, down_w).reshape(rows.shape)
    return (output, select, weight)


def per_device(
    residual_input,
    attention_norm_gain,
    receptance_weight,
    key_weight,
    value_weight,
    decay_weight,
    correction_rate_weight,
    output_gate_weight,
    decay_offset,
    correction_rate_offset,
    self_term_weight,
    head_read_gain,
    previous_state,
    attention_output_weight,
    feedforward_norm_gain,
    routes,
    routing_weight,
    routed_gate_weight,
    routed_up_weight,
    routed_down_weight,
    common_gate_weight,
    common_up_weight,
    common_down_weight,
):
    ep_size = lax.axis_size("ep")
    device = lax.axis_index("ep")
    tally_value = residual_input.shape[0]
    normed = rms_norm(residual_input.astype(jnp.float32), attention_norm_gain)
    stacked = jnp.stack(
        (
            receptance_weight,
            key_weight,
            value_weight,
            decay_weight,
            correction_rate_weight,
            output_gate_weight,
        ),
        axis=1,
    )
    local_cols = jnp.einsum(
        "td,drc->trc",
        lax.all_gather(normed, "ep", axis=0, tiled=True),
        stacked,
        preferred_element_type=jnp.float32,
    ).astype(jnp.bfloat16)
    role_rows = lax.all_to_all(local_cols, "ep", split_axis=0, concat_axis=2, tiled=True)
    normed_mixer_input, next_state = attention_mixer(
        role_rows[:, 0],
        role_rows[:, 1],
        role_rows[:, 2],
        role_rows[:, 3],
        role_rows[:, 4],
        role_rows[:, 5],
        decay_offset,
        correction_rate_offset,
        self_term_weight,
        head_read_gain,
        previous_state,
    )
    attended = jnp.dot(
        normed_mixer_input, attention_output_weight, preferred_element_type=jnp.float32
    ).astype(jnp.bfloat16)
    middle = residual_input.astype(jnp.float32) + attended.astype(jnp.float32)
    normed_ffn = rms_norm(middle, feedforward_norm_gain)
    shared = expert_mlp(normed_ffn, common_gate_weight, common_up_weight, common_down_weight)
    expert_count = routed_gate_weight.shape[0] * ep_size
    all_ids = jnp.arange(expert_count, dtype=jnp.int32)
    own_ids = device.reshape(1)
    own_routes = lax.dynamic_slice_in_dim(routes, device * tally_value, tally_value, 0)
    own_weight = lax.dynamic_slice_in_dim(routing_weight, device * tally_value, tally_value, 0)
    whole = lax.all_gather(normed_ffn, "ep", axis=0, tiled=True)
    output, unused_select, unused_weight = serve_gathered(
        whole,
        routes,
        routing_weight,
        ep_size,
        tally_value,
        own_ids,
        routed_gate_weight[0],
        routed_up_weight[0],
        routed_down_weight[0],
    )
    returned = lax.all_to_all(output, "ep", split_axis=0, concat_axis=0, tiled=True)
    select, weight = slot_table(own_routes, own_weight, all_ids)
    routed = combine_returned(select, weight, returned)
    hidden_out = (middle + shared.astype(jnp.float32) + routed).astype(jnp.bfloat16)
    return (hidden_out, next_state)


def solution(mesh):
    return jax.shard_map(
        per_device,
        mesh=mesh,
        in_specs=(
            P(("grp", "ep"), None),
            P(),
            P(None, "ep"),
            P(None, "ep"),
            P(None, "ep"),
            P(None, "ep"),
            P(None, "ep"),
            P(None, "ep"),
            P(),
            P(),
            P(),
            P(),
            P(("grp", "ep"), None, None),
            P(),
            P(),
            P("grp", None),
            P("grp", None),
            P("ep", None, None),
            P("ep", None, None),
            P("ep", None, None),
            P(),
            P(),
            P(),
        ),
        out_specs=(P(("grp", "ep"), None), P(("grp", "ep"), None, None)),
        check_vma=False,
    )
```

profile of v0, /device:TPU:0, one launch (start us, length us, event | category | flops | bytes accessed | tf_op | source)
XLA Modules:
  0.0 249.9 jit_solution(6900193728107449112)
XLA Ops:
  7.2 0.8 convert_element_type.171
  8.1 1.0 fusion.34
  9.1 1.6 fusion.36
  10.7 0.9 bitcast_dynamic-update-slice_fusion.5
  11.7 0.9 bitcast_dynamic-update-slice_fusion.4
  12.6 0.9 bitcast_dynamic-update-slice_fusion.3
  13.5 0.9 bitcast_dynamic-update-slice_fusion.2
  14.4 0.9 bitcast_dynamic-update-slice_fusion.1
  15.3 0.9 bitcast_dynamic-update-slice_fusion
  16.3 57.0 %all-gather.3.cloned.1.call-done = bf16[768,2048]{1,0:T(8,128)(2,1)} async-done(((bf16[24,2048]{1,0:T(8,128)(2,1)}), bf16[768,2048]{1,0:T(8,128)(2,1)}) %all-gather.3.cloned.1.call-update) | async-done | bytes 3145744 | tf_op jit(solution)/shard_map/all_gather | solution.py:159
  73.2 3.1 %fusion.72 = f32[768,192]{0,1:S(1)} fusion(bf16[768,2048]{1,0:T(8,128)(2,1)} %all-gather.3.cloned.1.call-done, bf16[2048,192]{0,1:T(8,128)(2,1)S(1)} %bitcast.99), kind=kOutput, calls=%fused_computation.110 | convolution fusion | flops 603979776 | bytes 4521984
  76.4 1.8 copy.38
  78.2 3.4 %reshape.259 = bf16[32,2,2304]{2,1,0:T(2,128)(2,1)} reshape(bf16[768,6,32]{2,1,0:T(8,128)(2,1)} %copy.38) | data formatting | bytes 589824
  81.6 3.3 %all-to-all-start = ((bf16[32,2,2304]{2,1,0:T(2,128)(2,1)}), bf16[32,2,2304]{2,1,0:T(2,128)(2,1)S(1)}, u32[]{:S(2)}, u32[]{:S(2)}) async-start(bf16[32,2,2304]{2,1,0:T(2,128)(2,1)} %reshape.259), calls=%async_computation | async-start | bytes 589824 | tf_op jit(solution)/shard_map/all_to_all | solution.py:163
  85.0 0.2 all-gather.5.cloned.1.call-start
  85.3 10.8 %reshape.237 = f32[24,16,64,64]{3,2,1,0:T(8,128)} reshape(f32[24,16,4096]{2,1,0:T(8,128)} %param.35) | data formatting | bytes 12582912 | tf_op jit(solution)/shard_map/reshape | solution.py:52
  96.4 2.2 reshape.260
  98.6 2.2 copy.40
  100.8 1.9 all_to_all.19
  102.7 0.9 slice_convert_fusion.2
  103.6 0.8 reshape.258
  105.1 0.2 fusion.41
  105.5 22.8 %fusion.73 = f32[24,16,1,64]{3,2,1,0:T(1,128)S(1)} fusion(f32[24,16,64,1]{2,3,1,0:T(1,128)S(1)} %bitcast.97, f32[24,16,64,64]{3,2,1,0:T(8,128)} %reshape.237), kind=kOutput, calls=%fused_computation.111 | convolution fusion | flops 18874368 | bytes 6488064 | tf_op jit(solution)/shard_map/nhvk,nhk->nhv/dot_general | solution.py:53
  128.3 16.5 %fusion.1 = f32[24,16,1,64]{3,2,1,0:T(1,128)S(1)} fusion(bf16[24,16,64,1]{2,3,1,0:T(2,128)(2,1)S(1)} %copy-done.6, f32[24,16,64,64]{3,2,1,0:T(8,128)S(1)} %copy-done.1, f32[24,16,64]{2,1,0:T(8,128)S(1)} %fusion.41, f32[24,16,64]{2,1,0:T(8,128)S(1)} %get-tuple-element.2, f32[24,16,64]{2,1,0:T(8,128)S(1)} %bitcast.95, f32[24,16,64]{2,1,0:T(8,128)S(1)} %get-tuple-element.4, ...), kind=kOutput, calls=%fused_computation.1 | convolution fusion | flops 26738688 | bytes 6930432 | tf_op jit(solution)/shard_map/nhvk,nhk->nhv/dot_general | solution.py:59
  144.9 0.2 multiply_reduce_fusion.1
  145.2 0.8 fusion.24
  146.1 3.0 %multiply_reduce_fusion = (f32[24]{0:T(128)S(1)}, f32[24,2048]{1,0:T(8,128)S(1)}) fusion(bf16[1024,2048]{1,0:T(8,128)(2,1)} %param.36, f32[24,1024]{1,0:T(8,128)S(1)} %reshape.239, bf16[24,6,1024]{2,0,1:T(8,128)(2,1)} %all_to_all.19, bf16[24,2048]{1,0:T(8,128)(2,1)S(1)} %copy-done.3), kind=kOutput, calls=%fused_computation.49 | convolution fusion | flops 101105640 | bytes 4636768 | tf_op jit(solution)/shard_map/dot_general | solution.py:177
  149.1 0.7 multiply_convert_fusion
  149.8 0.7 compare_reduce_fusion
  150.7 0.2 reduce_window_sum.23
  150.9 0.8 constant_dynamic-slice_fusion.1
  151.8 0.8 constant_dynamic-slice_fusion
  152.5 0.7 select_reduce_fusion
  153.2 9.3 %broadcast_multiply_fusion = (f32[24,16,64,64]{3,2,1,0:T(8,128)}, f32[24,16,64,64]{3,2,1,0:T(8,128)}) fusion(f32[24,16,64]{2,1,0:T(8,128)S(1)} %get-tuple-element.4, f32[24,16,64]{2,1,0:T(8,128)S(1)} %reshape.246, f32[24,16,64]{2,1,0:T(8,128)S(1)} %get-tuple-element.2, f32[24,16,64]{2,1,0:T(8,128)S(1)} %bitcast.96), kind=kLoop, calls=%fused_computation.6 | loop fusion | flops 3145728 | bytes 12976128 | tf_op jit(solution)/shard_map/mul | solution.py:57
  162.5 10.8 %mul.247 = f32[24,16,4096]{2,1,0:T(8,128)} reshape(f32[24,16,64,64]{3,2,1,0:T(8,128)} %get-tuple-element.14) | data formatting | bytes 12582912 | tf_op jit(solution)/shard_map/mul | solution.py:57
  173.3 10.9 %mul.246 = f32[24,16,4096]{2,1,0:T(8,128)} reshape(f32[24,16,64,64]{3,2,1,0:T(8,128)} %get-tuple-element.15) | data formatting | bytes 12582912 | tf_op jit(solution)/shard_map/mul | solution.py:56
  184.3 5.4 %mul.206 = f32[24,16,64,64]{3,2,1,0:T(8,128)} broadcast(f32[24,16,64]{2,1,0:T(8,128)S(1)} %copy-done.5), dimensions={0,1,3} | broadcast | bytes 6389760 | tf_op jit(solution)/shard_map/mul | solution.py:55
  189.6 10.9 %mul.244 = f32[24,16,4096]{2,1,0:T(8,128)} reshape(f32[24,16,64,64]{3,2,1,0:T(8,128)} %mul.206) | data formatting | bytes 12582912 | tf_op jit(solution)/shard_map/mul | solution.py:55
  200.6 9.7 %all-gather.5.cloned.1.call-done = bf16[768,2048]{1,0:T(8,128)(2,1)} async-done(((bf16[24,2048]{1,0:T(8,128)(2,1)}), bf16[768,2048]{1,0:T(8,128)(2,1)}) %all-gather.5.cloned.1.call-update) | async-done | bytes 3145744 | tf_op jit(solution)/shard_map/all_gather | solution.py:188
  210.3 2.7 %convolution_convert_fusion.1 = bf16[32,4,2048]{2,1,0:T(4,128)(2,1)S(1)} fusion(bf16[32,24,2048]{2,1,0:T(8,128)(2,1)} %bitcast.91, s32[32,24]{1,0:T(8,128)S(1)} %sub.39, pred[32,24]{1,0:T(8,128)(4,1)S(1)} %broadcast_compare_fusion), kind=kOutput, calls=%fused_computation.10 | convolution fusion | flops 12857344 | bytes 3673856 | tf_op jit(solution)/shard_map/snc,snd->scd/dot_general | solution.py:107
  213.1 2.7 %fusion.15 = f32[128,512]{1,0:T(8,128)} fusion(bf16[128,2048]{1,0:T(8,128)(2,1)S(1)} %reshape.241, bf16[1,2048,512]{2,1,0:T(8,128)(2,1)} %param.40), kind=kOutput, calls=%fused_computation.23 | convolution fusion | flops 268435456 | bytes 2883584 | tf_op jit(solution)/shard_map/dot_general | solution.py:17
  215.8 2.4 convolution_convert_fusion
  218.3 1.0 reshape.242
  219.2 3.3 %all-to-all-start.1 = ((bf16[32,4,2048]{2,1,0:T(4,128)(2,1)}), bf16[32,4,2048]{2,1,0:T(4,128)(2,1)S(1)}, u32[]{:S(2)}, u32[]{:S(2)}) async-start(bf16[32,4,2048]{2,1,0:T(4,128)(2,1)} %reshape.242), calls=%async_computation.1 | async-start | bytes 1048576 | tf_op jit(solution)/shard_map/all_to_all | solution.py:200
  222.6 14.2 %subtract_add_fusion = f32[24,16,4096]{2,1,0:T(8,128)} fusion(f32[24,16,4096]{2,1,0:T(8,128)} %mul.247, f32[24,16,4096]{2,1,0:T(8,128)} %mul.246, f32[24,16,4096]{2,1,0:T(8,128)} %param.35, f32[24,16,4096]{2,1,0:T(8,128)} %mul.244), kind=kLoop, calls=%fused_computation.5 | loop fusion | flops 4718592 | bytes 31457280 | tf_op jit(solution)/shard_map/add | solution.py:55
  236.8 2.0 fusion.74
  238.8 3.0 %fusion.9 = f32[24,2048]{1,0:T(8,128)S(1)} fusion(f32[24,2048]{1,0:T(8,128)S(1)} %get-tuple-element.13, bf16[512,2048]{1,0:T(8,128)(2,1)} %param.45, bf16[24,2048]{1,0:T(8,128)(2,1)S(1)} %copy-done.2, bf16[2048,512]{1,0:T(8,128)(2,1)} %param.44, f32[24,512]{1,0:T(8,128)S(1)} %fusion.74), kind=kOutput, calls=%fused_computation.16 | convolution fusion | flops 100884480 | bytes 4734976 | tf_op jit(solution)/shard_map/dot_general | solution.py:20
  241.8 1.3 fusion.7
  (60 shorter events, 1.8 us)
Async XLA Ops:
  7.2 208.7 %copy-start = (bf16[1,512,2048]{2,1,0:T(8,128)(2,1)S(1)}, bf16[1,512,2048]{2,1,0:T(8,128)(2,1)}, u32[]{:S(2)}) copy-start(bf16[1,512,2048]{2,1,0:T(8,128)(2,1)} %param.42) | copy-start | bytes 6291460
  7.2 66.1 %all-gather.3.cloned.1.call-start = ((), (), s32[]{:S(2)}) async-start(), calls=%async_computation.2 | async-start | bytes 3244032 | tf_op jit(solution)/shard_map/all_gather | solution.py:159
  81.6 14.8 %all-to-all-start = ((bf16[32,2,2304]{2,1,0:T(2,128)(2,1)}), bf16[32,2,2304]{2,1,0:T(2,128)(2,1)S(1)}, u32[]{:S(2)}, u32[]{:S(2)}) async-start(bf16[32,2,2304]{2,1,0:T(2,128)(2,1)} %reshape.259), calls=%async_computation | async-start | bytes 589824 | tf_op jit(solution)/shard_map/all_to_all | solution.py:163
  85.0 11.1 %copy-start.8 = (f32[1024]{0:T(1024)S(1)}, f32[1024]{0:T(1024)}, u32[]{:S(2)}) copy-start(f32[1024]{0:T(1024)} %param.31) | copy-start | bytes 12292
  85.0 11.2 %copy-start.9 = (f32[1024]{0:T(1024)S(1)}, f32[1024]{0:T(1024)}, u32[]{:S(2)}) copy-start(f32[1024]{0:T(1024)} %param.32) | copy-start | bytes 12292
  85.0 11.3 %copy-start.10 = (f32[1024]{0:T(1024)S(1)}, f32[1024]{0:T(1024)}, u32[]{:S(2)}) copy-start(f32[1024]{0:T(1024)} %param.33) | copy-start | bytes 12292
  85.0 11.3 %copy-start.11 = (f32[1024]{0:T(1024)S(1)}, f32[1024]{0:T(1024)}, u32[]{:S(2)}) copy-start(f32[1024]{0:T(1024)} %param.34) | copy-start | bytes 12292
  85.0 11.4 %copy-start.12 = (bf16[2048]{0:T(1024)(128)(2,1)S(1)}, bf16[2048]{0:T(1024)(128)(2,1)}, u32[]{:S(2)}) copy-start(bf16[2048]{0:T(1024)(128)(2,1)} %param.37) | copy-start | bytes 12292
  85.0 125.3 %all-gather.5.cloned.1.call-start = ((), (), s32[]{:S(2)}) async-start(), calls=%async_computation.3 | async-start | bytes 3244032 | tf_op jit(solution)/shard_map/all_gather | solution.py:188
  105.3 22.9 %copy-start.4 = (f32[24,16,64]{2,1,0:T(8,128)}, f32[24,16,64]{2,1,0:T(8,128)S(1)}, u32[]{:S(2)}) copy-start(f32[24,16,64]{2,1,0:T(8,128)S(1)} %fusion.41) | copy-start | bytes 294916
  105.5 22.8 %copy-start.1 = (f32[24,16,64,64]{3,2,1,0:T(8,128)S(1)}, f32[24,16,64,64]{3,2,1,0:T(8,128)}, u32[]{:S(2)}) copy-start(f32[24,16,64,64]{3,2,1,0:T(8,128)} %reshape.237) | copy-start | bytes 18874372
  105.5 22.8 %copy-start.6 = (bf16[24,16,64,1]{2,3,1,0:T(2,128)(2,1)S(1)}, bf16[24,16,64,1]{2,3,1,0:T(2,128)(2,1)}, u32[]{:S(2)}) copy-start(bf16[24,16,64,1]{2,3,1,0:T(2,128)(2,1)} %reshape.258) | copy-start | bytes 147460
  128.3 17.8 %copy-start.3 = (bf16[24,2048]{1,0:T(8,128)(2,1)S(1)}, bf16[24,2048]{1,0:T(8,128)(2,1)}, u32[]{:S(2)}) copy-start(bf16[24,2048]{1,0:T(8,128)(2,1)} %param.23) | copy-start | bytes 294916
  173.3 10.9 %copy-start.5 = (f32[24,16,64]{2,1,0:T(8,128)S(1)}, f32[24,16,64]{2,1,0:T(8,128)}, u32[]{:S(2)}) copy-start(f32[24,16,64]{2,1,0:T(8,128)} %copy-done.4) | copy-start | bytes 294916
  219.2 22.5 %all-to-all-start.1 = ((bf16[32,4,2048]{2,1,0:T(4,128)(2,1)}), bf16[32,4,2048]{2,1,0:T(4,128)(2,1)S(1)}, u32[]{:S(2)}, u32[]{:S(2)}) async-start(bf16[32,4,2048]{2,1,0:T(4,128)(2,1)} %reshape.242), calls=%async_computation.1 | async-start | bytes 1048576 | tf_op jit(solution)/shard_map/all_to_all | solution.py:200
  222.6 14.2 %copy-start.2 = (bf16[24,2048]{1,0:T(8,128)(2,1)S(1)}, bf16[24,2048]{1,0:T(8,128)(2,1)}, u32[]{:S(2)}) copy-start(bf16[24,2048]{1,0:T(8,128)(2,1)} %multiply_convert_fusion) | copy-start | bytes 294916
  236.8 5.0 %copy-start.7 = (f32[24,32]{1,0:T(8,128)S(1)}, f32[24,32]{1,0:T(8,128)}, u32[]{:S(2)}) copy-start(f32[24,32]{1,0:T(8,128)} %select_reduce_fusion) | copy-start | bytes 9220
Sparse Core Ops, SparseCore 0:
  11.4 61.7 all-gather.2
  150.0 60.2 all-gather.4
where the time goes:
time: 251 us; the launch traced here: 250 us
  local copies, waits for them, and re-layouts  70.5 us (28%)
  waiting for transfers between devices  66.8 us (27%)
  matrix products  59.4 us (24%)
  other arithmetic  32 us (13%)
  between operations  14.4 us (6%)
  starting transfers between devices  6.93 us (3%)
    all_gather x1, waiting for transfers between devices, per_device(): lax.all_gather(normed, 'ep', axis=0, tiled=True)  57 us
    dot_general x1, matrix products, attention_mixer(): jnp.einsum('nhvk,nhk->nhv', matrix, unit_key, precision=lax.Precision.HIG...  22.8 us
    dot_general x1, matrix products, attention_mixer(): jnp.einsum('nhvk,nhk->nhv', matrix, receptance_head, precision=lax.Precis...  16.5 us
    mul x2, local copies, waits for them, and re-layouts, attention_mixer(): matrix * heads(decay)[:, :, None, :]  16.3 us
    add x1, other arithmetic, attention_mixer(): matrix * heads(decay)[:, :, None, :]  14.2 us
    mul x1, local copies, waits for them, and re-layouts, attention_mixer(): recalled[..., None] * removal[:, :, None, :]  10.9 us
    reshape x1, local copies, waits for them, and re-layouts, attention_mixer(): matrix = head_state.reshape(tally_value, HEAD_COUNT, HEAD_SIZE, HEAD_SIZE)  10.8 us
    mul x1, local copies, waits for them, and re-layouts, attention_mixer(): head_value[..., None] * rate_scaled_key[:, :, None, :]  10.8 us
  transfers between devices with their start and end apart: 4, of which 2 were waited for; matrix products, arithmetic and copies ran while one was open for 35% of the time, Pallas kernels for 0%

commit v1 on v0

v1 whole, which is shorter than its diff:
```python
import functools
import math

import jax
import jax.numpy as jnp
import numpy as np
from jax import lax
from jax.experimental import pallas as pl
from jax.experimental.pallas import tpu as pltpu
from jax.sharding import PartitionSpec as P

HEAD_COUNT = 16
HEAD_SIZE = 64
CAP = 4
ROLES = 6
LANES = 128
F32 = jnp.float32
BF16 = jnp.bfloat16


def rms_norm(value_rows, gain):
    scale = lax.rsqrt(jnp.mean(value_rows * value_rows, axis=-1, keepdims=True) + 1e-06)
    return (value_rows * scale * gain.astype(F32)).astype(BF16)


def expert_mlp(rows, gate_w, up_w, down_w):
    gate = jnp.dot(rows, gate_w, preferred_element_type=F32)
    upward = jnp.dot(rows, up_w, preferred_element_type=F32)
    hidden = (jax.nn.silu(gate) * upward).astype(BF16)
    return jnp.dot(hidden, down_w, preferred_element_type=F32).astype(BF16)


def place_matrices(pieces):
    width = HEAD_SIZE // pieces
    place = np.zeros((pieces, ROLES * width, ROLES * LANES), np.float32)
    for piece in range(pieces):
        for role in range(ROLES):
            for column in range(width):
                for copy in range(LANES // HEAD_SIZE):
                    lane = role * LANES + copy * HEAD_SIZE + piece * width + column
                    place[piece, role * width + column, lane] = 1.0
    return place


def split(value):
    high = value.astype(BF16)
    return high, (value - high.astype(F32)).astype(BF16)


def dot(a, b):
    return jnp.dot(a, b, preferred_element_type=F32)


def mixer_kernel(
    land_ref, place_ref, spread_ref, gather_ref, block_ref, consts_ref, state_ref, out_w_ref,
    resid_ref, gain_ref, select_ref,
    next_ref, middle_ref, normed_ref, rows_ref,
    role_ref, mixed_ref,
):
    step = pl.program_id(0)
    tokens = land_ref.shape[1]
    pieces = place_ref.shape[0]
    step_rows = state_ref.shape[0] * HEAD_COUNT

    @pl.when(step == 0)
    def _():
        for head in range(HEAD_COUNT):
            total = dot(land_ref[head * pieces], place_ref[0])
            for piece in range(1, pieces):
                total = total + dot(land_ref[head * pieces + piece], place_ref[piece])
            for number in range(ROLES):
                part = total[:, number * LANES : (number + 1) * LANES]
                role_ref[number, pl.ds(head, tokens, stride=HEAD_COUNT), :] = part

    base = pl.multiple_of(step * step_rows, step_rows)

    def role(number):
        return role_ref[number, pl.ds(base, step_rows), :]

    def const(number):
        one = consts_ref[number]
        return jnp.concatenate([one] * state_ref.shape[0], axis=0)

    half = HEAD_SIZE / LANES

    def head_sum(value):
        return jnp.sum(value, axis=-1, keepdims=True) * half

    receptance, keys, values = role(0), role(1), role(2)
    decay = jnp.exp(-math.exp(-0.5) * jax.nn.sigmoid(const(0) + role(3)))
    rate = jax.nn.sigmoid(const(1) + role(4))
    unit_key = keys * lax.rsqrt(1.0 + head_sum(keys * keys))
    scaled_key = keys * rate
    removal = unit_key * rate
    self_sum = head_sum(receptance * scaled_key * const(2))

    def twice(value):
        return jnp.concatenate([value, value], axis=1)

    unit_key2, decay2, removal2 = twice(unit_key), twice(decay), twice(removal)
    scaled_key2, receptance2 = twice(scaled_key), twice(receptance)
    values_b = values[:, :HEAD_SIZE].astype(BF16)
    block = block_ref[...]
    chunk = block.shape[0]
    read = jnp.zeros((step_rows, LANES), F32)
    group = state_ref.shape[0]
    for c in range(HEAD_SIZE * HEAD_SIZE // chunk):
        cols = slice(c * chunk, (c + 1) * chunk)
        state = state_ref[:, :, cols].reshape(step_rows, chunk)
        high, low = split(state * unit_key2)
        recalled = dot(high, block) + dot(low, block)
        spread = dot(values_b, spread_ref[:, cols])
        new = state * decay2 - recalled * removal2 + spread * scaled_key2
        next_ref[:, :, cols] = new.reshape(group, HEAD_COUNT, chunk)
        high, low = split(new * receptance2)
        pick = gather_ref[cols, :]
        read = read + dot(high, pick) + dot(low, pick)
    centered = read - head_sum(read) * (1.0 / HEAD_SIZE)
    variance = head_sum(centered * centered) * (1.0 / HEAD_SIZE)
    normal = centered * lax.rsqrt(variance + 0.00064) * const(3)
    mixed_ref[pl.ds(base, step_rows), :] = (normal + self_sum * values) * jax.nn.sigmoid(role(5))

    @pl.when(step == pl.num_programs(0) - 1)
    def _():
        lane = lax.broadcasted_iota(jnp.int32, (tokens, LANES), 1)
        per = LANES // HEAD_SIZE
        parts = []
        for first in range(0, HEAD_COUNT, per):
            part = mixed_ref[pl.ds(first, tokens, stride=HEAD_COUNT), :]
            for other in range(1, per):
                rest = mixed_ref[pl.ds(first + other, tokens, stride=HEAD_COUNT), :]
                part = jnp.where(lane < other * HEAD_SIZE, part, rest)
            parts.append(part.astype(BF16))
        mixed = jnp.concatenate(parts, axis=1)
        attended = dot(mixed, out_w_ref[...]).astype(BF16).astype(F32)
        middle = resid_ref[...].astype(F32) + attended
        middle_ref[...] = middle
        normed = rms_norm(middle, gain_ref[...])
        normed_ref[...] = normed
        rows_ref[...] = dot(select_ref[...], normed).astype(BF16)


def mixer(land, consts, state, out_w, resid, gain, select):
    sources, tokens, width = land.shape
    pieces = sources // HEAD_COUNT
    model = resid.shape[1]
    group = 8 if tokens % 8 == 0 else 1
    chunk = 4 * HEAD_SIZE
    place = jnp.asarray(place_matrices(pieces), BF16)
    eye = np.eye(HEAD_SIZE, dtype=np.float32)
    spread = jnp.asarray(np.repeat(eye, HEAD_SIZE, axis=1), BF16)
    gather = jnp.asarray(np.repeat(np.concatenate([eye] * (LANES // HEAD_SIZE), 1), HEAD_SIZE, 0), BF16)
    block = jnp.asarray(np.kron(np.eye(chunk // HEAD_SIZE), np.ones((HEAD_SIZE, HEAD_SIZE))), BF16)
    full = lambda array: pl.BlockSpec(array.shape, lambda i: (0,) * array.ndim)
    state_spec = pl.BlockSpec((group,) + state.shape[1:], lambda i: (i, 0, 0))
    operands = (land, place, spread, gather, block, consts, state, out_w, resid, gain, select)
    specs = [full(a) for a in operands]
    specs[6] = state_spec
    whole = lambda shape: pl.BlockSpec(shape, lambda i: (0,) * len(shape))
    slots = select.shape[0]
    return pl.pallas_call(
        mixer_kernel,
        grid=(tokens // group,),
        out_shape=(
            jax.ShapeDtypeStruct(state.shape, F32),
            jax.ShapeDtypeStruct((tokens, model), F32),
            jax.ShapeDtypeStruct((tokens, model), BF16),
            jax.ShapeDtypeStruct((slots, model), BF16),
        ),
        in_specs=specs,
        out_specs=(state_spec, whole((tokens, model)), whole((tokens, model)), whole((slots, model))),
        scratch_shapes=[
            pltpu.VMEM((ROLES, tokens * HEAD_COUNT, LANES), F32),
            pltpu.VMEM((tokens * HEAD_COUNT, LANES), F32),
        ],
        compiler_params=pltpu.CompilerParams(vmem_limit_bytes=50 * 1024 * 1024),
        cost_estimate=pl.CostEstimate(flops=4_000_000_000, bytes_accessed=20_000_000, transcendentals=0),
    )(*operands)


def per_device(
    residual_input,
    attention_norm_gain,
    receptance_weight,
    key_weight,
    value_weight,
    decay_weight,
    correction_rate_weight,
    output_gate_weight,
    decay_offset,
    correction_rate_offset,
    self_term_weight,
    head_read_gain,
    previous_state,
    attention_output_weight,
    feedforward_norm_gain,
    routes,
    routing_weight,
    routed_gate_weight,
    routed_up_weight,
    routed_down_weight,
    common_gate_weight,
    common_up_weight,
    common_down_weight,
):
    ep_size = lax.axis_size("ep")
    device = lax.axis_index("ep")
    tokens, model = residual_input.shape
    normed = rms_norm(residual_input.astype(F32), attention_norm_gain)
    stacked = jnp.concatenate(
        (
            receptance_weight,
            key_weight,
            value_weight,
            decay_weight,
            correction_rate_weight,
            output_gate_weight,
        ),
        axis=1,
    )
    own_routes = lax.dynamic_slice_in_dim(routes, device * tokens, tokens, 0)
    own_weight = lax.dynamic_slice_in_dim(routing_weight, device * tokens, tokens, 0)
    experts = routed_gate_weight.shape[0] * ep_size
    match = own_routes[:, :, None] == jnp.arange(experts, dtype=jnp.int32)
    hit = jnp.any(match, axis=1)
    weight = jnp.sum(jnp.where(match, own_weight[:, :, None], 0.0), axis=1)
    rank = jnp.cumsum(hit.astype(jnp.int32), axis=0) - hit.astype(jnp.int32)
    chosen = hit[:, :, None] & (rank[:, :, None] == jnp.arange(CAP, dtype=jnp.int32))
    select = chosen.astype(BF16).reshape(tokens, experts * CAP)
    coefficient = jnp.where(chosen, weight[:, :, None], 0.0).reshape(tokens, experts * CAP)
    coef_high, coef_low = split(coefficient)

    cols = dot(lax.all_gather(normed, "ep", axis=0, tiled=True), stacked).astype(BF16)
    land = lax.all_to_all(
        cols.reshape(ep_size, tokens, cols.shape[-1]), "ep", split_axis=0, concat_axis=0, tiled=True
    )
    by_head = jnp.stack((decay_offset, correction_rate_offset, self_term_weight, head_read_gain))
    by_head = by_head.reshape(4, HEAD_COUNT, HEAD_SIZE)
    consts = jnp.concatenate([by_head] * (LANES // HEAD_SIZE), axis=-1)
    next_state, middle, normed_ffn, rows = mixer(
        land,
        consts,
        previous_state,
        attention_output_weight,
        residual_input,
        feedforward_norm_gain.reshape(1, model),
        select.T,
    )
    served = lax.all_to_all(
        rows.reshape(ep_size, -1, model), "ep", split_axis=0, concat_axis=0, tiled=True
    )
    shared = expert_mlp(normed_ffn, common_gate_weight, common_up_weight, common_down_weight)
    output = expert_mlp(
        served.reshape(-1, model),
        routed_gate_weight[0],
        routed_up_weight[0],
        routed_down_weight[0],
    )
    returned = lax.all_to_all(
        output.reshape(ep_size, -1, model), "ep", split_axis=0, concat_axis=0, tiled=True
    ).reshape(-1, model)
    routed = dot(
        jnp.concatenate((coef_high, coef_low), axis=0), returned
    )
    routed = routed[:tokens] + routed[tokens:]
    hidden_out = (middle + shared.astype(F32) + routed).astype(BF16)
    return (hidden_out, next_state)


def solution(mesh):
    return jax.shard_map(
        per_device,
        mesh=mesh,
        in_specs=(
            P(("grp", "ep"), None),
            P(),
            P(None, "ep"),
            P(None, "ep"),
            P(None, "ep"),
            P(None, "ep"),
            P(None, "ep"),
            P(None, "ep"),
            P(),
            P(),
            P(),
            P(),
            P(("grp", "ep"), None, None),
            P(),
            P(),
            P("grp", None),
            P("grp", None),
            P("ep", None, None),
            P("ep", None, None),
            P("ep", None, None),
            P(),
            P(),
            P(),
        ),
        out_specs=(P(("grp", "ep"), None), P(("grp", "ep"), None, None)),
        check_vma=False,
    )
```

time: 251 us -> 177 us (0.71)
  local copies, waits for them, and re-layouts: 70.5 us -> 19 us
  matrix products: 59.4 us -> 14.2 us
  other arithmetic: 32 us -> 4.53 us
  blocking collectives: 0 us -> 18.9 us
  Pallas kernels: 0 us -> 18.7 us
  waiting for transfers between devices: 66.8 us -> 79.7 us
    dot_general x9 -> x6, matrix products: 56.3 us -> 14.2 us  [the longest x2 6.83 us: expert_mlp(): return jnp.dot(hidden, down_w, preferred_element_type=F32).astype(BF16)]
    mul x6 -> x0, local copies, waits for them, and re-layouts: 38.2 us -> none  [the longest x2 16.3 us: attention_mixer(): matrix * heads(decay)[:, :, None, :]]
    all_to_all x2, waiting for transfers between devices: 0.01 us -> 24.4 us  [the longest x1 13.4 us: per_device(): lax.all_to_all(output.reshape(ep_size, -1, model), 'ep', split_axis=0, co...]
    all_to_all x0 -> x1, blocking collectives: none -> 18.9 us  [per_device(): lax.all_to_all(rows.reshape(ep_size, -1, model), 'ep', split_axis=0, conc...]
    pallas_call x0 -> x1, Pallas kernels: none -> 18.7 us  [mixer(): pl.pallas_call(mixer_kernel, grid=(tokens // group,), out_shape=(jax.Shap...]
    add x1 -> x0, other arithmetic: 14.2 us -> none  [attention_mixer(): matrix * heads(decay)[:, :, None, :]]
    mul x3 -> x0, other arithmetic: 10.2 us -> none  [the longest x1 9.28 us: attention_mixer(): head_value[..., None] * rate_scaled_key[:, :, None, :]]
    all_gather x1 -> x0, waiting for transfers between devices: 9.72 us -> none  [per_device(): whole = lax.all_gather(normed_ffn, 'ep', axis=0, tiled=True)]
  transfers between devices with their start and end apart: 4 -> 3, of which waited for: 2 -> 3; matrix products, arithmetic and copies ran while one was open for 35% -> 6% of each run, Pallas kernels for 0% -> 0%
where the time goes in v1:
time: 177 us; the launch traced here: 176 us
  waiting for transfers between devices  79.7 us (45%)
  local copies, waits for them, and re-layouts  19 us (11%)
  blocking collectives  18.9 us (11%)
  Pallas kernels  18.7 us (11%)
  between operations  14.3 us (8%)
  matrix products  14.2 us (8%)
  starting transfers between devices  6.7 us (4%)
  other arithmetic  4.53 us (3%)
    all_gather x1, waiting for transfers between devices, per_device(): lax.all_gather(normed, 'ep', axis=0, tiled=True)  55.3 us
    all_to_all x1, blocking collectives, per_device(): lax.all_to_all(rows.reshape(ep_size, -1, model), 'ep', split_axis=0, conc...  18.9 us
    pallas_call x1, Pallas kernels, mixer(): pl.pallas_call(mixer_kernel, grid=(tokens // group,), out_shape=(jax.Shap...  18.7 us
    all_to_all x1, waiting for transfers between devices, per_device(): lax.all_to_all(output.reshape(ep_size, -1, model), 'ep', split_axis=0, co...  13.4 us
    all_to_all x1, waiting for transfers between devices, per_device(): lax.all_to_all(cols.reshape(ep_size, tokens, cols.shape[-1]), 'ep', split...  11 us
    unnamed x33, local copies, waits for them, and re-layouts  9.45 us
    dot_general x2, matrix products, expert_mlp(): return jnp.dot(hidden, down_w, preferred_element_type=F32).astype(BF16)  6.83 us
    dot_general x2, matrix products, expert_mlp(): gate = jnp.dot(rows, gate_w, preferred_element_type=F32)  4.04 us
  transfers between devices with their start and end apart: 3, of which 3 were waited for; matrix products, arithmetic and copies ran while one was open for 6% of the time, Pallas kernels for 0%

profile of v1, /device:TPU:0, one launch (start us, length us, event | category | flops | bytes accessed | tf_op | source)
XLA Modules:
  0.0 175.9 jit_solution(6633217248953880067)
XLA Ops:
  7.2 1.2 fusion.23
  8.4 0.7 convert_element_type.54
  9.1 1.6 fusion.25
  10.7 0.8 constant_dynamic-slice_fusion.1
  11.5 0.1 fusion.32
  11.7 0.8 constant_dynamic-slice_fusion
  12.4 0.9 constant_dynamic-update-slice_fusion.5
  13.3 0.9 constant_dynamic-update-slice_fusion.4
  14.3 0.9 constant_dynamic-update-slice_fusion.3
  15.2 0.9 constant_dynamic-update-slice_fusion.2
  16.1 0.9 constant_dynamic-update-slice_fusion.1
  17.0 0.9 constant_dynamic-update-slice_fusion
  18.0 55.3 %all-gather.2.cloned.1.call-done = bf16[768,2048]{1,0:T(8,128)(2,1)} async-done(((bf16[24,2048]{1,0:T(8,128)(2,1)}), bf16[768,2048]{1,0:T(8,128)(2,1)}) %all-gather.2.cloned.1.call-update) | async-done | bytes 3145744 | tf_op jit(solution)/shard_map/all_gather | solution.py:233
  73.3 3.1 %convolution_convert_fusion.2 = bf16[768,192]{0,1:T(8,128)(2,1)S(1)} fusion(bf16[768,2048]{1,0:T(8,128)(2,1)} %all-gather.2.cloned.1.call-done, bf16[2048,192]{0,1:T(8,128)(2,1)S(1)} %constant_dynamic-update-slice_fusion), kind=kOutput, calls=%fused_computation.11 | convolution fusion | flops 604127232 | bytes 4227072 | tf_op jit(solution)/shard_map/dot_general | solution.py:51
  76.4 0.9 copy.52
  77.3 3.3 %all-to-all-start = ((bf16[32,24,192]{2,1,0:T(8,128)(2,1)}), bf16[32,24,192]{2,1,0:T(8,128)(2,1)S(1)}, u32[]{:S(2)}, u32[]{:S(2)}) async-start(bf16[32,24,192]{2,1,0:T(8,128)(2,1)} %bitcast), calls=%async_computation | async-start | bytes 786432 | tf_op jit(solution)/shard_map/all_to_all | solution.py:234
  80.6 0.1 select_reduce_fusion
  80.7 0.1 copy.53
  80.8 0.1 copy.55
  80.9 0.1 stack.15
  81.0 0.1 stack.16
  81.0 0.1 stack.17
  81.1 0.1 stack.18
  81.2 0.1 copy.54
  81.3 0.1 eq.40
  81.4 0.1 maximum_maximum_fusion.consts_ref
  81.5 0.7 select_convert_fusion
  82.3 0.6 copy-done.6
  82.8 11.0 %all-to-all-done.land_ref = bf16[32,24,192]{2,1,0:T(8,128)(2,1)S(1)} async-done(((bf16[32,24,192]{2,1,0:T(8,128)(2,1)}), bf16[32,24,192]{2,1,0:T(8,128)(2,1)S(1)}, u32[]{:S(2)}, u32[]{:S(2)}) %all-to-all-start) | async-done | bytes 294944 | tf_op jit(solution)/shard_map/all_to_all | solution.py:234
  93.9 1.2 copy-done.2
  95.1 1.1 copy-done.3
  96.2 1.0 copy-done.4
  97.2 0.9 copy-done.5
  98.1 18.7 %shard_map.266 = (f32[24,16,4096]{2,1,0:T(8,128)}, f32[24,2048]{1,0:T(8,128)S(1)}, bf16[24,2048]{1,0:T(8,128)(2,1)S(1)}, bf16[128,2048]{1,0:T(8,128)(2,1)S(1)}) custom-call(bf16[32,24,192]{2,1,0:T(8,128)(2,1)S(1)} %all-to-all-done.land_ref, bf16[2,192,768]{2,1,0:T(8,128)(2,1)S(1)} %copy-done.3, bf16[64,4096]{1,0:T(8,128)(2,1)S(1)} %copy-done.4, ...), custom_call_target="tpu_custom_call" | custom-call | flops 4000000000 | bytes 20000000 | tf_op jit(solution)/shard_map/pallas_call | solution.py:161
  116.8 1.0 reshape.67
  117.8 18.9 %all_to_all.15 = bf16[32,4,2048]{2,1,0:T(4,128)(2,1)} all-to-all(bf16[32,4,2048]{2,1,0:T(4,128)(2,1)} %reshape.67), channel_id=1, replica_groups=mesh['grp'=1,'ep'=32] {'ep'}, dimensions={0} | all-to-all | bytes 1048576 | tf_op jit(solution)/shard_map/all_to_all | solution.py:249
  136.7 1.2 reshape.68
  137.9 2.0 %fusion.7 = f32[128,512]{1,0:T(8,128)S(1)} fusion(bf16[128,2048]{1,0:T(8,128)(2,1)S(1)} %reshape.68, bf16[1,2048,512]{2,1,0:T(8,128)(2,1)} %param.44), kind=kOutput, calls=%fused_computation.9 | convolution fusion | flops 268435456 | bytes 2883584 | tf_op jit(solution)/shard_map/dot_general | solution.py:27
  139.9 3.2 %convolution_convert_fusion = bf16[128,2048]{1,0:T(8,128)(2,1)} fusion(bf16[1,512,2048]{2,1,0:T(8,128)(2,1)S(1)} %copy-done, bf16[128,2048]{1,0:T(8,128)(2,1)S(1)} %reshape.68, bf16[1,2048,512]{2,1,0:T(8,128)(2,1)} %param.45, f32[128,512]{1,0:T(8,128)S(1)} %fusion.7), kind=kOutput, calls=%fused_computation | convolution fusion | flops 537526272 | bytes 5505024 | tf_op jit(solution)/shard_map/dot_general | solution.py:30
  143.1 2.0 %reshape.69 = bf16[32,4,2048]{2,1,0:T(4,128)(2,1)} reshape(bf16[128,2048]{1,0:T(8,128)(2,1)} %convolution_convert_fusion) | data formatting | bytes 1048576 | tf_op jit(solution)/shard_map/reshape | solution.py:260
  145.2 3.3 %all-to-all-start.2 = ((bf16[32,4,2048]{2,1,0:T(4,128)(2,1)}), bf16[32,4,2048]{2,1,0:T(4,128)(2,1)}, u32[]{:S(2)}, u32[]{:S(2)}) async-start(bf16[32,4,2048]{2,1,0:T(4,128)(2,1)} %reshape.69), calls=%async_computation.2 | async-start | bytes 1048576 | tf_op jit(solution)/shard_map/all_to_all | solution.py:259
  148.5 0.1 copy.57
  148.6 0.1 copy.56
  148.7 2.0 %fusion.41 = f32[24,512]{1,0:T(8,128)S(1)} fusion(bf16[24,2048]{1,0:T(8,128)(2,1)S(1)} %get-tuple-element.7, bf16[2048,512]{1,0:T(8,128)(2,1)} %param.47), kind=kOutput, calls=%fused_computation.59 | convolution fusion | flops 50331648 | bytes 2244608 | tf_op jit(solution)/shard_map/dot_general | solution.py:27
  150.7 13.4 %all-to-all-done.2 = bf16[32,4,2048]{2,1,0:T(4,128)(2,1)} async-done(((bf16[32,4,2048]{2,1,0:T(4,128)(2,1)}), bf16[32,4,2048]{2,1,0:T(4,128)(2,1)}, u32[]{:S(2)}, u32[]{:S(2)}) %all-to-all-start.2) | async-done | bytes 524320 | tf_op jit(solution)/shard_map/all_to_all | solution.py:259
  164.1 1.2 reshape.70
  165.3 0.2 fusion.34
  165.5 3.6 %fusion.3 = bf16[24,2048]{1,0:T(8,128)(2,1)} fusion(f32[24,2048]{1,0:T(8,128)S(1)} %get-tuple-element.6, bf16[512,2048]{1,0:T(8,128)(2,1)} %param.49, bf16[24,2048]{1,0:T(8,128)(2,1)S(1)} %get-tuple-element.7, bf16[2048,512]{1,0:T(8,128)(2,1)} %param.48, f32[48,2048]{1,0:T(8,128)S(1)} %fusion.34, f32[24,512]{1,0:T(8,128)S(1)} %fusion.41), kind=kOutput, calls=%fused_computation.5 | convolution fusion | flops 101031936 | bytes 5029888 | tf_op jit(solution)/shard_map/dot_general | solution.py:30
  (36 shorter events, 0.3 us)
Async XLA Ops:
  7.2 132.8 %copy-start = (bf16[1,512,2048]{2,1,0:T(8,128)(2,1)S(1)}, bf16[1,512,2048]{2,1,0:T(8,128)(2,1)}, u32[]{:S(2)}) copy-start(bf16[1,512,2048]{2,1,0:T(8,128)(2,1)} %param.46) | copy-start | bytes 6291460
  7.2 66.1 %all-gather.2.cloned.1.call-start = ((), (), s32[]{:S(2)}) async-start(), calls=%async_computation.3 | async-start | bytes 3244032 | tf_op jit(solution)/shard_map/all_gather | solution.py:233
  17.9 63.0 %copy-start.9 = (f32[1024]{0:T(1024)S(1)}, f32[1024]{0:T(1024)}, u32[]{:S(2)}) copy-start(f32[1024]{0:T(1024)} %param.35) | copy-start | bytes 12292
  17.9 63.0 %copy-start.10 = (f32[1024]{0:T(1024)S(1)}, f32[1024]{0:T(1024)}, u32[]{:S(2)}) copy-start(f32[1024]{0:T(1024)} %param.36) | copy-start | bytes 12292
  18.0 63.1 %copy-start.11 = (f32[1024]{0:T(1024)S(1)}, f32[1024]{0:T(1024)}, u32[]{:S(2)}) copy-start(f32[1024]{0:T(1024)} %param.37) | copy-start | bytes 12292
  18.0 63.1 %copy-start.12 = (f32[1024]{0:T(1024)S(1)}, f32[1024]{0:T(1024)}, u32[]{:S(2)}) copy-start(f32[1024]{0:T(1024)} %param.38) | copy-start | bytes 12292
  18.0 63.2 %copy-start.13 = (bf16[2048]{0:T(1024)(128)(2,1)S(1)}, bf16[2048]{0:T(1024)(128)(2,1)}, u32[]{:S(2)}) copy-start(bf16[2048]{0:T(1024)(128)(2,1)} %param.41) | copy-start | bytes 12292
  76.3 17.5 %copy-start.1 = (bf16[24,2048]{1,0:T(8,128)(2,1)S(1)}, bf16[24,2048]{1,0:T(8,128)(2,1)}, u32[]{:S(2)}) copy-start(bf16[24,2048]{1,0:T(8,128)(2,1)} %resid_ref.1) | copy-start | bytes 294916
  77.3 16.6 %all-to-all-start = ((bf16[32,24,192]{2,1,0:T(8,128)(2,1)}), bf16[32,24,192]{2,1,0:T(8,128)(2,1)S(1)}, u32[]{:S(2)}, u32[]{:S(2)}) async-start(bf16[32,24,192]{2,1,0:T(8,128)(2,1)} %bitcast), calls=%async_computation | async-start | bytes 786432 | tf_op jit(solution)/shard_map/all_to_all | solution.py:234
  82.2 0.6 copy-start.6
  93.9 1.2 copy-start.2
  95.1 1.1 copy-start.3
  96.2 1.0 copy-start.4
  97.2 0.9 copy-start.5
  143.1 5.4 %copy-start.7 = (pred[24,128]{0,1:T(8,128)(4,1)S(1)}, pred[24,128]{0,1:T(8,128)(4,1)}, u32[]{:S(2)}) copy-start(pred[24,128]{0,1:T(8,128)(4,1)} %copy-done.6) | copy-start | bytes 9220
  143.1 5.5 %copy-start.8 = (bf16[24,128]{0,1:T(8,128)(2,1)S(1)}, bf16[24,128]{0,1:T(8,128)(2,1)}, u32[]{:S(2)}) copy-start(bf16[24,128]{0,1:T(8,128)(2,1)} %get-tuple-element.10) | copy-start | bytes 18436
  145.2 18.9 %all-to-all-start.2 = ((bf16[32,4,2048]{2,1,0:T(4,128)(2,1)}), bf16[32,4,2048]{2,1,0:T(4,128)(2,1)}, u32[]{:S(2)}, u32[]{:S(2)}) async-start(bf16[32,4,2048]{2,1,0:T(4,128)(2,1)} %reshape.69), calls=%async_computation.2 | async-start | bytes 1048576 | tf_op jit(solution)/shard_map/all_to_all | solution.py:259
Sparse Core Ops, SparseCore 0:
  11.4 61.7 all-gather.1

commit v2 on v1

--- a/solution.py
+++ b/solution.py
@@ -178,6 +178,158 @@
     )(*operands)
 
 
+PLANE = 8
+
+
+def project_kernel(
+    depth, normed_ref, w0, w1, w2, w3, w4, w5, land_out,
+    weight_ref, held, cols, land,
+    z_send, z_recv, near_send, near_recv, half_send, half_recv, core_send, core_recv,
+    out_send, out_recv,
+):
+    total = depth * PLANE
+    tokens, model = normed_ref.shape
+    cut = model // 2
+    me = lax.axis_index("ep")
+    core = lax.rem(me, 2)
+    x = lax.rem(me // 2, 2)
+    y = lax.rem(me // 4, 2)
+    along_x = me + 2 - 4 * x
+    along_y = me + 4 - 8 * y
+    mate = me + 1 - 2 * core
+    plane = lax.rem(me, PLANE)
+    plane_x, plane_y, plane_c = lax.rem(along_x, PLANE), lax.rem(along_y, PLANE), lax.rem(mate, PLANE)
+    far = lax.rem(along_x + 4 - 8 * y, PLANE)
+    level = me // PLANE
+
+    def send(source, target, device, send_sem, recv_sem):
+        copy = pltpu.make_async_remote_copy(
+            src_ref=source, dst_ref=target, send_sem=send_sem, recv_sem=recv_sem,
+            device_id={"ep": device}, device_id_type=pl.DeviceIdType.MESH,
+        )
+        copy.start()
+        return copy
+
+    def slot(of_plane, d):
+        return held.at[of_plane, lax.rem(level + depth - d, depth)]
+
+    sent = []
+    along_z = [None]
+    for d in range(1, depth):
+        there = lax.rem(me + PLANE * d, total)
+        along_z.append(send(normed_ref, slot(plane, 0), there, z_send.at[d], z_recv.at[d]))
+    by_y, by_x, by_core = [], [], [[], [], [], []]
+    for d in range(depth):
+        if d:
+            along_z[d].wait_recv()
+        source = normed_ref if d == 0 else slot(plane, d)
+        here = slot(plane, d)
+        by_y.append(send(source, here, along_y, near_send.at[0, d], near_recv.at[0, d]))
+        by_x.append(send(source, here, along_x, near_send.at[1, d], near_recv.at[1, d]))
+        by_core[0].append(send(source, here, mate, core_send.at[0, d], core_recv.at[0, d]))
+        if d == 0:
+            held[plane, level] = normed_ref[...]
+            weight_ref[...] = jnp.concatenate(
+                [w[...] for w in (w0, w1, w2, w3, w4, w5)], axis=1
+            )
+
+    def compute(group):
+        rows = held[group].astype(F32).reshape(depth * tokens, model).astype(BF16)
+        result = dot(rows, weight_ref[...]).astype(BF16).astype(F32)
+        cols[group] = result.reshape(depth, tokens, result.shape[-1]).astype(BF16)
+
+    def give(group):
+        for z in range(depth):
+            to = z * PLANE + group
+            number = lax.rem(to - me + total, total)
+
+            @pl.when(to != me)
+            def _():
+                send(cols.at[group, z], land.at[me], to, out_send.at[number], out_recv.at[number])
+
+            @pl.when(to == me)
+            def _():
+                land[me] = cols[group, z]
+
+    compute(plane)
+    halves = []
+    for d in range(depth):
+        by_y[d].wait_recv()
+        block = held.at[plane_y, lax.rem(level + depth - d, depth)]
+        first = block.at[:, :cut]
+        halves.append(send(first, first, along_x, half_send.at[0, d], half_recv.at[0, d]))
+        by_core[1].append(send(block, block, mate, core_send.at[1, d], core_recv.at[1, d]))
+        by_x[d].wait_recv()
+        block = held.at[plane_x, lax.rem(level + depth - d, depth)]
+        second = block.at[:, cut:]
+        halves.append(send(second, second, along_y, half_send.at[1, d], half_recv.at[1, d]))
+        by_core[2].append(send(block, block, mate, core_send.at[2, d], core_recv.at[2, d]))
+    compute(plane_y)
+    give(plane)
+    compute(plane_x)
+    give(plane_y)
+    for d in range(depth):
+        halves[2 * d].wait_recv()
+        halves[2 * d + 1].wait_recv()
+        block = slot(far, d)
+        by_core[3].append(send(block, block, mate, core_send.at[3, d], core_recv.at[3, d]))
+    before = plane_x
+    compute(far)
+    give(before)
+    before = far
+    for which, group in enumerate((plane, plane_y, plane_x, far)):
+        for d in range(depth):
+            by_core[which][d].wait_recv()
+        other = group + 1 - 2 * core
+        compute(other)
+        give(before)
+        before = other
+    give(before)
+    for copy in along_z[1:] + by_y + by_x + halves + by_core[0] + by_core[1] + by_core[2] + by_core[3]:
+        copy.wait_send()
+
+    def finish(number, carry):
+        copy = pltpu.make_async_remote_copy(
+            src_ref=cols.at[0, 0], dst_ref=land.at[0],
+            send_sem=out_send.at[number], recv_sem=out_recv.at[number],
+            device_id={"ep": lax.rem(me + number, total)}, device_id_type=pl.DeviceIdType.MESH,
+        )
+        copy.wait_recv()
+        copy.wait_send()
+        return carry
+
+    lax.fori_loop(1, total, finish, 0)
+    land_out[...] = land[...]
+
+
+def project(normed, weights, ep_size):
+    depth = ep_size // PLANE
+    tokens, model = normed.shape
+    width = sum(w.shape[1] for w in weights)
+    dma = pltpu.SemaphoreType.DMA
+    return pl.pallas_call(
+        functools.partial(project_kernel, depth),
+        out_shape=jax.ShapeDtypeStruct((ep_size, tokens, width), BF16),
+        in_specs=[pl.BlockSpec(memory_space=pltpu.VMEM)] * 7,
+        out_specs=pl.BlockSpec(memory_space=pltpu.VMEM),
+        scratch_shapes=[
+            pltpu.VMEM((model, width), BF16),
+            pltpu.VMEM((PLANE, depth, tokens, model), BF16),
+            pltpu.VMEM((PLANE, depth, tokens, width), BF16),
+            pltpu.VMEM((ep_size, tokens, width), BF16),
+            dma((depth,)), dma((depth,)),
+            dma((2, depth)), dma((2, depth)),
+            dma((2, depth)), dma((2, depth)),
+            dma((4, depth)), dma((4, depth)),
+            dma((ep_size,)), dma((ep_size,)),
+        ],
+        compiler_params=pltpu.CompilerParams(
+            has_side_effects=True, vmem_limit_bytes=40 * 1024 * 1024
+        ),
+        cost_estimate=pl.CostEstimate(flops=600_000_000, bytes_accessed=100_000_000, transcendentals=0),
+    )(normed, *weights)
+
+
 def per_device(
     residual_input,
     attention_norm_gain,
@@ -207,17 +359,6 @@
     device = lax.axis_index("ep")
     tokens, model = residual_input.shape
     normed = rms_norm(residual_input.astype(F32), attention_norm_gain)
-    stacked = jnp.concatenate(
-        (
-            receptance_weight,
-            key_weight,
-            value_weight,
-            decay_weight,
-            correction_rate_weight,
-            output_gate_weight,
-        ),
-        axis=1,
-    )
     own_routes = lax.dynamic_slice_in_dim(routes, device * tokens, tokens, 0)
     own_weight = lax.dynamic_slice_in_dim(routing_weight, device * tokens, tokens, 0)
     experts = routed_gate_weight.shape[0] * ep_size
@@ -230,9 +371,17 @@
     coefficient = jnp.where(chosen, weight[:, :, None], 0.0).reshape(tokens, experts * CAP)
     coef_high, coef_low = split(coefficient)
 
-    cols = dot(lax.all_gather(normed, "ep", axis=0, tiled=True), stacked).astype(BF16)
-    land = lax.all_to_all(
-        cols.reshape(ep_size, tokens, cols.shape[-1]), "ep", split_axis=0, concat_axis=0, tiled=True
+    land = project(
+        normed,
+        (
+            receptance_weight,
+            key_weight,
+            value_weight,
+            decay_weight,
+            correction_rate_weight,
+            output_gate_weight,
+        ),
+        ep_size,
     )
     by_head = jnp.stack((decay_offset, correction_rate_offset, self_term_weight, head_read_gain))
     by_head = by_head.reshape(4, HEAD_COUNT, HEAD_SIZE)

time: 177 us -> 131 us (0.74)
  waiting for transfers between devices: 79.7 us -> 13.4 us
  Pallas kernels: 18.7 us -> 56.6 us
  between operations: 14.3 us -> 0.84 us
  local copies, waits for them, and re-layouts: 19 us -> 22.9 us
  starting transfers between devices: 6.7 us -> 2.98 us
  matrix products: 14.2 us -> 11 us
    all_gather x1 -> x0, waiting for transfers between devices: 55.3 us -> none  [per_device(): lax.all_gather(normed, 'ep', axis=0, tiled=True)]
    pallas_call x0 -> x1, Pallas kernels: none -> 37.9 us  [project(): pl.pallas_call(functools.partial(project_kernel, depth), out_shape=jax.Sh...]
    all_to_all x1 -> x0, waiting for transfers between devices: 11 us -> none  [per_device(): lax.all_to_all(cols.reshape(ep_size, tokens, cols.shape[-1]), 'ep', split...]
    another operation x4, local copies, waits for them, and re-layouts: 0.28 us -> 4.21 us  [per_device(): jnp.stack((decay_offset, correction_rate_offset, self_term_weight, head_r...]
    unnamed x33 -> x28, local copies, waits for them, and re-layouts: 9.45 us -> 13.3 us
    all_to_all x1 -> x0, starting transfers between devices: 3.33 us -> none  [per_device(): lax.all_to_all(cols.reshape(ep_size, tokens, cols.shape[-1]), 'ep', split...]
    dot_general x2 -> x1, matrix products: 3.28 us -> 0.21 us  [dot(): return jnp.dot(a, b, preferred_element_type=F32)]
  transfers between devices with their start and end apart: 3 -> 1, of which waited for: 3 -> 1; matrix products, arithmetic and copies ran while one was open for 6% -> 2% of each run, Pallas kernels for 0% -> 0%
where the time goes in v2:
time: 131 us
  Pallas kernels  56.6 us (43%)
  local copies, waits for them, and re-layouts  22.9 us (17%)
  blocking collectives  18.4 us (14%)
  waiting for transfers between devices  13.4 us (10%)
  matrix products  11 us (8%)
  other arithmetic  4.33 us (3%)
  starting transfers between devices  2.98 us (2%)
    pallas_call x1, Pallas kernels, project(): pl.pallas_call(functools.partial(project_kernel, depth), out_shape=jax.Sh...  37.9 us
    pallas_call x1, Pallas kernels, mixer(): pl.pallas_call(mixer_kernel, grid=(tokens // group,), out_shape=(jax.Shap...  18.7 us
    all_to_all x1, blocking collectives, per_device(): lax.all_to_all(rows.reshape(ep_size, -1, model), 'ep', split_axis=0, conc...  18.4 us
    all_to_all x1, waiting for transfers between devices, per_device(): lax.all_to_all(output.reshape(ep_size, -1, model), 'ep', split_axis=0, co...  13.4 us
    unnamed x28, local copies, waits for them, and re-layouts  13.3 us
    dot_general x2, matrix products, expert_mlp(): return jnp.dot(hidden, down_w, preferred_element_type=F32).astype(BF16)  6.04 us
    dot_general x2, matrix products, expert_mlp(): gate = jnp.dot(rows, gate_w, preferred_element_type=F32)  4.73 us
    another operation x4, local copies, waits for them, and re-layouts, per_device(): jnp.stack((decay_offset, correction_rate_offset, self_term_weight, head_r...  4.21 us
  transfers between devices with their start and end apart: 1, of which 1 were waited for; matrix products, arithmetic and copies ran while one was open for 2% of the time, Pallas kernels for 0%

profile of v2, /device:TPU:0, one launch (start us, length us, event | category | flops | bytes accessed | tf_op | source)
XLA Modules:
  0.0 130.5 jit_solution(15666908908733982183)
XLA Ops:
  0.6 0.0 copy-start
  0.6 0.9 constant_dynamic-slice_fusion.1
  1.6 0.1 fusion.32
  1.6 0.1 copy.78
  1.7 1.0 fusion.23
  2.8 0.6 add_rsqrt_fusion
  3.4 0.8 constant_dynamic-slice_fusion
  4.1 0.1 select_reduce_fusion
  4.2 0.1 copy.80
  4.3 0.7 convert_element_type.51
  5.0 0.8 stack.15
  5.8 0.8 stack.16
  6.5 1.3 %stack.17 = f32[1,16,64]{2,1,0:T(8,128)} reshape(f32[1024]{0:T(1024)} %param.37) | data formatting | bytes 8192 | tf_op jit(solution)/shard_map/stack | solution.py:386
  7.9 1.4 %stack.18 = f32[1,16,64]{2,1,0:T(8,128)} reshape(f32[1024]{0:T(1024)} %param.38) | data formatting | bytes 8192 | tf_op jit(solution)/shard_map/stack | solution.py:386
  9.2 0.7 reshape.62.gain_ref
  10.0 0.1 copy.79
  10.0 0.1 eq.40
  10.2 0.0 copy-start.5
  10.2 0.1 select_convert_fusion
  10.3 0.0 copy-start.10
  10.4 1.2 copy.72.w0
  11.6 1.2 copy.73.w1
  12.8 1.9 %copy.74.w2 = bf16[2048,32]{1,0:T(8,128)(2,1)} copy(bf16[2048,32]{0,1:T(8,128)(2,1)} %param.31) | data formatting | bytes 262144 | tf_op args[4]
  14.7 1.0 copy.75.w3
  15.7 1.9 %copy.76.w4 = bf16[2048,32]{1,0:T(8,128)(2,1)} copy(bf16[2048,32]{0,1:T(8,128)(2,1)} %param.33) | data formatting | bytes 262144 | tf_op args[6]
  17.6 1.9 %copy.77.w5 = bf16[2048,32]{1,0:T(8,128)(2,1)} copy(bf16[2048,32]{0,1:T(8,128)(2,1)} %param.34) | data formatting | bytes 262144 | tf_op args[7]
  19.5 0.8 fusion.25.normed_ref
  20.3 0.9 maximum_maximum_fusion.consts_ref
  21.2 1.0 copy-done.1
  22.2 1.0 copy-done.2
  23.3 1.0 copy-done.3
  24.3 1.0 copy-done.4
  25.3 37.9 %shard_map.266.land_ref = bf16[32,24,192]{2,1,0:T(8,128)(2,1)S(1)} custom-call(bf16[24,2048]{1,0:T(8,128)(2,1)S(1)} %fusion.25.normed_ref, bf16[2048,32]{1,0:T(8,128)(2,1)S(1)} %copy.72.w0, bf16[2048,32]{1,0:T(8,128)(2,1)S(1)} %copy.73.w1, bf16[2048,32]{1,0:T(8,128)(2,1)S(1)} %copy-done.1, bf16[2048,32]{1,0:T(8,128)(2,1)S(1)} %copy-done.2, ...), custom_call_target="tpu_custom_call" | custom-call | flops 600000000 | bytes 100000000 | tf_op jit(solution)/shard_map/pallas_call | solution.py:310
  63.3 18.7 %shard_map.267 = (f32[24,16,4096]{2,1,0:T(8,128)}, f32[24,2048]{1,0:T(8,128)S(1)}, bf16[24,2048]{1,0:T(8,128)(2,1)S(1)}, bf16[128,2048]{1,0:T(8,128)(2,1)S(1)}) custom-call(bf16[32,24,192]{2,1,0:T(8,128)(2,1)S(1)} %shard_map.266.land_ref, bf16[2,192,768]{2,1,0:T(8,128)(2,1)S(1)} %copy-done.7, bf16[64,4096]{1,0:T(8,128)(2,1)S(1)} %copy-done.8, ...), custom_call_target="tpu_custom_call" | custom-call | flops 4000000000 | bytes 20000000 | tf_op jit(solution)/shard_map/pallas_call | solution.py:161
  82.0 0.2 reshape.63
  82.2 18.4 %all_to_all.10 = bf16[32,4,2048]{2,1,0:T(4,128)(2,1)} all-to-all(bf16[32,4,2048]{2,1,0:T(4,128)(2,1)S(1)} %reshape.63), channel_id=1, replica_groups=mesh['grp'=1,'ep'=32] {'ep'}, dimensions={0} | all-to-all | bytes 1048576 | tf_op jit(solution)/shard_map/all_to_all | solution.py:398
  100.6 1.2 reshape.64
  101.8 2.7 %fusion.7 = f32[128,512]{1,0:T(8,128)} fusion(bf16[128,2048]{1,0:T(8,128)(2,1)S(1)} %reshape.64, bf16[1,2048,512]{2,1,0:T(8,128)(2,1)} %param.44), kind=kOutput, calls=%fused_computation.9 | convolution fusion | flops 268435456 | bytes 2883584 | tf_op jit(solution)/shard_map/dot_general | solution.py:27
  104.5 2.4 %convolution_convert_fusion = bf16[128,2048]{1,0:T(8,128)(2,1)S(1)} fusion(bf16[1,512,2048]{2,1,0:T(8,128)(2,1)S(1)} %copy-done, bf16[128,2048]{1,0:T(8,128)(2,1)S(1)} %reshape.64, bf16[1,2048,512]{2,1,0:T(8,128)(2,1)} %param.45, f32[128,512]{1,0:T(8,128)} %fusion.7), kind=kOutput, calls=%fused_computation | convolution fusion | flops 537526272 | bytes 5505024 | tf_op jit(solution)/shard_map/dot_general | solution.py:30
  106.9 1.0 reshape.65
  107.9 3.0 %all-to-all-start.1 = ((bf16[32,4,2048]{2,1,0:T(4,128)(2,1)}), bf16[32,4,2048]{2,1,0:T(4,128)(2,1)S(1)}, u32[]{:S(2)}, u32[]{:S(2)}) async-start(bf16[32,4,2048]{2,1,0:T(4,128)(2,1)} %reshape.65), calls=%async_computation.1 | async-start | bytes 1048576 | tf_op jit(solution)/shard_map/all_to_all | solution.py:408
  110.9 0.1 copy.82
  111.0 0.1 copy.81
  111.1 2.0 %fusion.41 = f32[24,512]{1,0:T(8,128)S(1)} fusion(bf16[24,2048]{1,0:T(8,128)(2,1)S(1)} %get-tuple-element.7, bf16[2048,512]{1,0:T(8,128)(2,1)} %param.47), kind=kOutput, calls=%fused_computation.52 | convolution fusion | flops 50331648 | bytes 2244608 | tf_op jit(solution)/shard_map/dot_general | solution.py:27
  113.1 13.4 %all-to-all-done.1 = bf16[32,4,2048]{2,1,0:T(4,128)(2,1)S(1)} async-done(((bf16[32,4,2048]{2,1,0:T(4,128)(2,1)}), bf16[32,4,2048]{2,1,0:T(4,128)(2,1)S(1)}, u32[]{:S(2)}, u32[]{:S(2)}) %all-to-all-start.1) | async-done | bytes 524320 | tf_op jit(solution)/shard_map/all_to_all | solution.py:408
  126.5 0.1 reshape.66
  126.7 0.2 fusion.34
  126.9 3.6 %fusion.3 = bf16[24,2048]{1,0:T(8,128)(2,1)} fusion(f32[24,2048]{1,0:T(8,128)S(1)} %get-tuple-element.6, bf16[512,2048]{1,0:T(8,128)(2,1)} %param.49, bf16[24,2048]{1,0:T(8,128)(2,1)S(1)} %get-tuple-element.7, bf16[2048,512]{1,0:T(8,128)(2,1)} %param.48, f32[48,2048]{1,0:T(8,128)S(1)} %fusion.34, f32[24,512]{1,0:T(8,128)S(1)} %fusion.41), kind=kOutput, calls=%fused_computation.5 | convolution fusion | flops 101031936 | bytes 5029888 | tf_op jit(solution)/shard_map/dot_general | solution.py:30
  (24 shorter events, 0.2 us)
Async XLA Ops:
  0.6 103.9 %copy-start = (bf16[1,512,2048]{2,1,0:T(8,128)(2,1)S(1)}, bf16[1,512,2048]{2,1,0:T(8,128)(2,1)}, u32[]{:S(2)}) copy-start(bf16[1,512,2048]{2,1,0:T(8,128)(2,1)} %param.46) | copy-start | bytes 6291460
  10.2 9.3 %copy-start.5 = (bf16[24,2048]{1,0:T(8,128)(2,1)S(1)}, bf16[24,2048]{1,0:T(8,128)(2,1)}, u32[]{:S(2)}) copy-start(bf16[24,2048]{1,0:T(8,128)(2,1)} %resid_ref.1) | copy-start | bytes 294916
  10.3 4.3 %copy-start.10 = (bf16[2048,32]{0,1:T(8,128)(2,1)S(1)}, bf16[2048,32]{0,1:T(8,128)(2,1)}, u32[]{:S(2)}) copy-start(bf16[2048,32]{0,1:T(8,128)(2,1)} %param.32) | copy-start | bytes 393220
  19.5 43.8 %copy-start.9 = (bf16[256,256]{1,0:T(8,128)(2,1)S(1)}, bf16[256,256]{1,0:T(8,128)(2,1)}, u32[]{:S(2)}) copy-start(bf16[256,256]{1,0:T(8,128)(2,1)} %constant.38.clone.block_ref) | copy-start | bytes 393220
  21.2 1.0 copy-start.1
  22.2 1.0 copy-start.2
  23.3 1.0 copy-start.3
  24.3 1.0 copy-start.4
  25.3 37.9 %copy-start.6 = (bf16[4096,128]{1,0:T(8,128)(2,1)S(1)}, bf16[4096,128]{1,0:T(8,128)(2,1)}, u32[]{:S(2)}) copy-start(bf16[4096,128]{1,0:T(8,128)(2,1)} %constant.37.clone.gather_ref) | copy-start | bytes 3145732
  25.3 37.9 %copy-start.7 = (bf16[2,192,768]{2,1,0:T(8,128)(2,1)S(1)}, bf16[2,192,768]{2,1,0:T(8,128)(2,1)}, u32[]{:S(2)}) copy-start(bf16[2,192,768]{2,1,0:T(8,128)(2,1)} %constant.35.clone.place_ref) | copy-start | bytes 1769476
  25.3 38.0 %copy-start.8 = (bf16[64,4096]{1,0:T(8,128)(2,1)S(1)}, bf16[64,4096]{1,0:T(8,128)(2,1)}, u32[]{:S(2)}) copy-start(bf16[64,4096]{1,0:T(8,128)(2,1)} %constant.36.clone.spread_ref) | copy-start | bytes 1572868
  107.9 18.6 %all-to-all-start.1 = ((bf16[32,4,2048]{2,1,0:T(4,128)(2,1)}), bf16[32,4,2048]{2,1,0:T(4,128)(2,1)S(1)}, u32[]{:S(2)}, u32[]{:S(2)}) async-start(bf16[32,4,2048]{2,1,0:T(4,128)(2,1)} %reshape.65), calls=%async_computation.1 | async-start | bytes 1048576 | tf_op jit(solution)/shard_map/all_to_all | solution.py:408

commit v3 on v2

--- a/solution.py
+++ b/solution.py
@@ -52,10 +52,10 @@
 
 
 def mixer_kernel(
-    land_ref, place_ref, spread_ref, gather_ref, block_ref, consts_ref, state_ref, out_w_ref,
+    land_ref, place_ref, spread_ref, gather_ref, block_ref, const0, const1, const2, const3, state_ref, out_w_ref,
     resid_ref, gain_ref, select_ref,
     next_ref, middle_ref, normed_ref, rows_ref,
-    role_ref, mixed_ref,
+    role_ref, mixed_ref, consts_ref,
 ):
     step = pl.program_id(0)
     tokens = land_ref.shape[1]
@@ -64,6 +64,13 @@
 
     @pl.when(step == 0)
     def _():
+        for number, source in enumerate((const0, const1, const2, const3)):
+            pair = source[...]
+            turned = pltpu.roll(pair, HEAD_SIZE, 1)
+            first = lax.broadcasted_iota(jnp.int32, pair.shape, 1) < HEAD_SIZE
+            count = pair.shape[0]
+            consts_ref[number, pl.ds(0, count, stride=2), :] = jnp.where(first, pair, turned)
+            consts_ref[number, pl.ds(1, count, stride=2), :] = jnp.where(first, turned, pair)
         for head in range(HEAD_COUNT):
             total = dot(land_ref[head * pieces], place_ref[0])
             for piece in range(1, pieces):
@@ -137,7 +144,7 @@
         middle_ref[...] = middle
         normed = rms_norm(middle, gain_ref[...])
         normed_ref[...] = normed
-        rows_ref[...] = dot(select_ref[...], normed).astype(BF16)
+        rows_ref[...] = dot(select_ref[...], normed).reshape(rows_ref.shape).astype(BF16)
 
 
 def mixer(land, consts, state, out_w, resid, gain, select):
@@ -153,9 +160,9 @@
     block = jnp.asarray(np.kron(np.eye(chunk // HEAD_SIZE), np.ones((HEAD_SIZE, HEAD_SIZE))), BF16)
     full = lambda array: pl.BlockSpec(array.shape, lambda i: (0,) * array.ndim)
     state_spec = pl.BlockSpec((group,) + state.shape[1:], lambda i: (i, 0, 0))
-    operands = (land, place, spread, gather, block, consts, state, out_w, resid, gain, select)
+    operands = (land, place, spread, gather, block, *consts, state, out_w, resid, gain, select)
     specs = [full(a) for a in operands]
-    specs[6] = state_spec
+    specs[9] = state_spec
     whole = lambda shape: pl.BlockSpec(shape, lambda i: (0,) * len(shape))
     slots = select.shape[0]
     return pl.pallas_call(
@@ -165,13 +172,14 @@
             jax.ShapeDtypeStruct(state.shape, F32),
             jax.ShapeDtypeStruct((tokens, model), F32),
             jax.ShapeDtypeStruct((tokens, model), BF16),
-            jax.ShapeDtypeStruct((slots, model), BF16),
+            jax.ShapeDtypeStruct((slots // CAP, CAP, model), BF16),
         ),
         in_specs=specs,
-        out_specs=(state_spec, whole((tokens, model)), whole((tokens, model)), whole((slots, model))),
+        out_specs=(state_spec, whole((tokens, model)), whole((tokens, model)), whole((slots // CAP, CAP, model))),
         scratch_shapes=[
             pltpu.VMEM((ROLES, tokens * HEAD_COUNT, LANES), F32),
             pltpu.VMEM((tokens * HEAD_COUNT, LANES), F32),
+            pltpu.VMEM((4, HEAD_COUNT, LANES), F32),
         ],
         compiler_params=pltpu.CompilerParams(vmem_limit_bytes=50 * 1024 * 1024),
         cost_estimate=pl.CostEstimate(flops=4_000_000_000, bytes_accessed=20_000_000, transcendentals=0),
@@ -230,12 +238,14 @@
         if d == 0:
             held[plane, level] = normed_ref[...]
             weight_ref[...] = jnp.concatenate(
-                [w[...] for w in (w0, w1, w2, w3, w4, w5)], axis=1
+                [w[...] for w in (w0, w1, w2, w3, w4, w5)], axis=0
             )
 
     def compute(group):
         rows = held[group].astype(F32).reshape(depth * tokens, model).astype(BF16)
-        result = dot(rows, weight_ref[...]).astype(BF16).astype(F32)
+        result = lax.dot_general(
+            rows, weight_ref[...], (((1,), (1,)), ((), ())), preferred_element_type=F32
+        )
         cols[group] = result.reshape(depth, tokens, result.shape[-1]).astype(BF16)
 
     def give(group):
@@ -305,7 +315,8 @@
 def project(normed, weights, ep_size):
     depth = ep_size // PLANE
     tokens, model = normed.shape
-    width = sum(w.shape[1] for w in weights)
+    weights = [w.T for w in weights]
+    width = sum(w.shape[0] for w in weights)
     dma = pltpu.SemaphoreType.DMA
     return pl.pallas_call(
         functools.partial(project_kernel, depth),
@@ -313,7 +324,7 @@
         in_specs=[pl.BlockSpec(memory_space=pltpu.VMEM)] * 7,
         out_specs=pl.BlockSpec(memory_space=pltpu.VMEM),
         scratch_shapes=[
-            pltpu.VMEM((model, width), BF16),
+            pltpu.VMEM((width, model), BF16),
             pltpu.VMEM((PLANE, depth, tokens, model), BF16),
             pltpu.VMEM((PLANE, depth, tokens, width), BF16),
             pltpu.VMEM((ep_size, tokens, width), BF16),
@@ -328,6 +339,113 @@
         ),
         cost_estimate=pl.CostEstimate(flops=600_000_000, bytes_accessed=100_000_000, transcendentals=0),
     )(normed, *weights)
+
+
+def experts_kernel(
+    depth, rows_ref, normed_ref, middle_ref, coef_ref, g0, g1, g2, g3, g4, g5, out_ref,
+    b0, b1, b2, b3, b4, b5, served, output, returned,
+    load_sem, go_send, go_recv, back_send, back_recv,
+):
+    total = depth * PLANE
+    tokens, model = normed_ref.shape
+    me = lax.axis_index("ep")
+    level = me // PLANE
+
+    def copy_of(source, target, device, send_sem, recv_sem):
+        return pltpu.make_async_remote_copy(
+            src_ref=source, dst_ref=target, send_sem=send_sem, recv_sem=recv_sem,
+            device_id={"ep": device}, device_id_type=pl.DeviceIdType.MESH,
+        )
+
+    def go(number):
+        to = lax.rem(me + number, total)
+        return copy_of(rows_ref.at[to], served.at[me], to, go_send.at[number], go_recv.at[number])
+
+    def back(to):
+        number = lax.rem(to - me + total, total)
+        return copy_of(
+            output.at[to], returned.at[me], to, back_send.at[number], back_recv.at[number]
+        )
+
+    def launch(number, carry):
+        go(number).start()
+        return carry
+
+    lax.fori_loop(1, total, launch, 0)
+    loads = [
+        pltpu.make_async_copy(source, target, load_sem.at[i])
+        for i, (source, target) in enumerate(zip((g0, g1, g2, g3, g4, g5), (b0, b1, b2, b3, b4, b5)))
+    ]
+    for load in loads:
+        load.start()
+    served[me] = rows_ref[me]
+    for load in loads[:3]:
+        load.wait()
+    shared = expert_mlp(normed_ref[...], b0[...], b1[...], b2[...])
+    partial = middle_ref[...] + shared.astype(F32)
+    for load in loads[3:]:
+        load.wait()
+
+    for d in range(depth):
+        first = lax.rem(level + depth - d, depth) * PLANE
+
+        def arrive(i, carry):
+            source = first + i
+
+            @pl.when(source != me)
+            def _():
+                go(lax.rem(me - source + total, total)).wait_recv()
+
+            return carry
+
+        lax.fori_loop(0, PLANE, arrive, 0)
+        rows = served[pl.ds(first, PLANE)].reshape(PLANE * CAP, model)
+        result = expert_mlp(rows, b3[...], b4[...], b5[...])
+        output[pl.ds(first, PLANE)] = result.reshape(PLANE, CAP, model)
+
+        def give(i, carry):
+            source = first + i
+
+            @pl.when(source != me)
+            def _():
+                back(source).start()
+
+            return carry
+
+        lax.fori_loop(0, PLANE, give, 0)
+    returned[me] = output[me]
+
+    def finish(number, carry):
+        go(number).wait_send()
+        ended = back(lax.rem(me + number, total))
+        ended.wait_recv()
+        ended.wait_send()
+        return carry
+
+    lax.fori_loop(1, total, finish, 0)
+    routed = dot(coef_ref[...], returned[...].reshape(total * CAP, model))
+    out_ref[...] = (partial + (routed[:tokens] + routed[tokens:])).astype(BF16)
+
+
+def experts_step(rows, normed, middle, coef, weights, ep_size):
+    depth = ep_size // PLANE
+    tokens, model = normed.shape
+    dma = pltpu.SemaphoreType.DMA
+    vmem = pl.BlockSpec(memory_space=pltpu.VMEM)
+    return pl.pallas_call(
+        functools.partial(experts_kernel, depth),
+        out_shape=jax.ShapeDtypeStruct((tokens, model), BF16),
+        in_specs=[vmem] * 4 + [pl.BlockSpec(memory_space=pl.ANY)] * 6,
+        out_specs=vmem,
+        scratch_shapes=[pltpu.VMEM(w.shape, BF16) for w in weights]
+        + [pltpu.VMEM(rows.shape, BF16)] * 3
+        + [dma((6,))]
+        + [dma((ep_size,))] * 4,
+        compiler_params=pltpu.CompilerParams(
+            has_side_effects=True, vmem_limit_bytes=40 * 1024 * 1024
+        ),
+        cost_estimate=pl.CostEstimate(flops=1_000_000_000, bytes_accessed=60_000_000, transcendentals=0),
+    )(rows, normed, middle, coef, *weights)
 
 
 def per_device(
@@ -383,9 +501,10 @@
         ),
         ep_size,
     )
-    by_head = jnp.stack((decay_offset, correction_rate_offset, self_term_weight, head_read_gain))
-    by_head = by_head.reshape(4, HEAD_COUNT, HEAD_SIZE)
-    consts = jnp.concatenate([by_head] * (LANES // HEAD_SIZE), axis=-1)
+    consts = [
+        c.reshape(-1, LANES)
+        for c in (decay_offset, correction_rate_offset, self_term_weight, head_read_gain)
+    ]
     next_state, middle, normed_ffn, rows = mixer(
         land,
         consts,
@@ -395,24 +514,21 @@
         feedforward_norm_gain.reshape(1, model),
         select.T,
     )
-    served = lax.all_to_all(
-        rows.reshape(ep_size, -1, model), "ep", split_axis=0, concat_axis=0, tiled=True
+    hidden_out = experts_step(
+        rows,
+        normed_ffn,
+        middle,
+        jnp.concatenate((coef_high, coef_low), axis=0),
+        (
+            common_gate_weight,
+            common_up_weight,
+            common_down_weight,
+            routed_gate_weight[0],
+            routed_up_weight[0],
+            routed_down_weight[0],
+        ),
+        ep_size,
     )
-    shared = expert_mlp(normed_ffn, common_gate_weight, common_up_weight, common_down_weight)
-    output = expert_mlp(
-        served.reshape(-1, model),
-        routed_gate_weight[0],
-        routed_up_weight[0],
-        routed_down_weight[0],
-    )
-    returned = lax.all_to_all(
-        output.reshape(ep_size, -1, model), "ep", split_axis=0, concat_axis=0, tiled=True
-    ).reshape(-1, model)
-    routed = dot(
-        jnp.concatenate((coef_high, coef_low), axis=0), returned
-    )
-    routed = routed[:tokens] + routed[tokens:]
-    hidden_out = (middle + shared.astype(F32) + routed).astype(BF16)
     return (hidden_out, next_state)
 
 

time: 131 us -> 108 us (0.82)
  Pallas kernels: 56.6 us -> 91.9 us
  blocking collectives: 18.4 us -> 0 us
  waiting for transfers between devices: 13.4 us -> 0 us
  local copies, waits for them, and re-layouts: 22.9 us -> 11.6 us
  matrix products: 11 us -> 0 us
  starting transfers between devices: 2.98 us -> 0 us
    pallas_call x0 -> x1, Pallas kernels: none -> 34.8 us  [experts_step(): pl.pallas_call(functools.partial(experts_kernel, depth), out_shape=jax.Sh...]
    all_to_all x1 -> x0, blocking collectives: 18.4 us -> none  [per_device(): lax.all_to_all(rows.reshape(ep_size, -1, model), 'ep', split_axis=0, conc...]
    all_to_all x1 -> x0, waiting for transfers between devices: 13.4 us -> none  [per_device(): lax.all_to_all(output.reshape(ep_size, -1, model), 'ep', split_axis=0, co...]
    dot_general x5 -> x0, matrix products: 11 us -> none  [the longest x2 6.04 us: expert_mlp(): return jnp.dot(hidden, down_w, preferred_element_type=F32).astype(BF16)]
    another operation x4 -> x0, local copies, waits for them, and re-layouts: 4.21 us -> none  [per_device(): jnp.stack((decay_offset, correction_rate_offset, self_term_weight, head_r...]
    unnamed x28 -> x45, local copies, waits for them, and re-layouts: 13.3 us -> 9.32 us
    all_to_all x1 -> x0, starting transfers between devices: 2.98 us -> none  [per_device(): lax.all_to_all(output.reshape(ep_size, -1, model), 'ep', split_axis=0, co...]
    reshape x4 -> x0, local copies, waits for them, and re-layouts: 2.46 us -> none  [the longest x1 1.16 us: per_device(): served.reshape(-1, model)]
  transfers between devices with their start and end apart: 1 -> 0, of which waited for: 1 -> 0; matrix products, arithmetic and copies ran while one was open for 2% -> 0% of each run, Pallas kernels for 0% -> 0%
where the time goes in v3:
time: 108 us
  Pallas kernels  91.9 us (85%)
  local copies, waits for them, and re-layouts  11.6 us (11%)
  other arithmetic  3.06 us (3%)
    pallas_call x1, Pallas kernels, project(): pl.pallas_call(functools.partial(project_kernel, depth), out_shape=jax.Sh...  38.2 us
    pallas_call x1, Pallas kernels, experts_step(): pl.pallas_call(functools.partial(experts_kernel, depth), out_shape=jax.Sh...  34.8 us
    pallas_call x1, Pallas kernels, mixer(): pl.pallas_call(mixer_kernel, grid=(tokens // group,), out_shape=(jax.Shap...  18.9 us
    unnamed x45, local copies, waits for them, and re-layouts  9.32 us

profile of v3, /device:TPU:0, one launch (start us, length us, event | category | flops | bytes accessed | tf_op | source)
XLA Modules:
  0.0 107.5 jit_solution(5959397097305926321)
XLA Ops:
  0.6 0.0 copy-start
  0.6 0.0 copy-start.21
  0.7 0.0 copy-start.19
  0.7 0.0 copy-start.7
  0.7 1.1 %fusion = f32[24]{0:T(128)S(1)} fusion(bf16[24,2048]{1,0:T(8,128)(2,1)} %resid_ref.1), kind=kLoop, calls=%fused_computation.2 | loop fusion | flops 147432 | bytes 98400 | tf_op jit(solution)/shard_map/reduce_sum | solution.py:22
  1.8 0.1 constant_dynamic-slice_fusion.1
  1.9 0.8 constant_dynamic-slice_fusion
  2.7 0.1 fusion.3
  2.8 0.1 copy.40
  2.9 0.1 select_reduce_fusion
  3.0 0.1 copy.45
  3.0 0.7 convert_element_type.33
  3.7 0.7 reshape.57.gain_ref
  4.4 0.1 copy.43
  4.6 0.1 copy.41
  4.7 0.1 eq.40
  4.8 0.1 copy.42
  4.9 0.1 copy.46
  5.0 0.1 copy.44.select_ref
  5.1 1.0 fusion.2.normed_ref
  6.1 0.0 copy-start.8
  6.1 0.9 copy-done.8
  7.0 0.9 copy-done.9
  7.9 0.9 copy-done.10
  8.8 0.9 copy-done.11
  9.7 0.9 copy-done.12
  10.6 0.9 copy-done.13
  11.6 38.2 %shard_map.266.land_ref = bf16[32,24,192]{2,1,0:T(8,128)(2,1)S(1)} custom-call(bf16[24,2048]{1,0:T(8,128)(2,1)S(1)} %fusion.2.normed_ref, bf16[32,2048]{1,0:T(8,128)(2,1)S(1)} %bitcast.21, bf16[32,2048]{1,0:T(8,128)(2,1)S(1)} %bitcast.22, bf16[32,2048]{1,0:T(8,128)(2,1)S(1)} %bitcast.23, bf16[32,2048]{1,0:T(8,128)(2,1)S(1)} %bitcast.24, ...), custom_call_target="tpu_custom_call" | custom-call | flops 600000000 | bytes 100000000 | tf_op jit(solution)/shard_map/pallas_call | solution.py:321
  49.8 0.0 copy-done.21
  49.8 0.0 copy-done.19
  49.8 0.0 copy-done.7
  49.8 0.0 copy-done.17
  49.8 0.0 copy-done.16
  49.8 0.0 copy-done.15
  49.8 0.0 copy-done.14
  49.8 0.0 copy-done.18
  49.8 0.0 copy-done.20
  49.9 0.0 copy-start.1
  49.9 0.0 copy-start.2
  49.9 0.0 copy-start.3
  49.9 0.0 copy-start.4
  49.9 18.9 %shard_map.267 = (f32[24,16,4096]{2,1,0:T(8,128)}, f32[24,2048]{1,0:T(8,128)S(1)}, bf16[24,2048]{1,0:T(8,128)(2,1)S(1)}, bf16[32,4,2048]{2,1,0:T(4,128)(2,1)S(1)}) custom-call(bf16[32,24,192]{2,1,0:T(8,128)(2,1)S(1)} %shard_map.266.land_ref, bf16[2,192,768]{2,1,0:T(8,128)(2,1)S(1)} %copy-done.19, bf16[64,4096]{1,0:T(8,128)(2,1)S(1)} %copy-done.20, ...), custom_call_target="tpu_custom_call" | custom-call | flops 4000000000 | bytes 20000000 | tf_op jit(solution)/shard_map/pallas_call | solution.py:168
  68.8 0.0 copy-done.2
  68.9 0.0 copy-start.5
  68.9 1.6 %copy-done.5 = bf16[1,2048,512]{2,1,0:T(8,128)(2,1)S(1)} copy-done((bf16[1,2048,512]{2,1,0:T(8,128)(2,1)S(1)}, bf16[1,2048,512]{2,1,0:T(8,128)(2,1)}, u32[]{:S(2)}) %copy-start.5) | copy-done | bytes 2097176
  70.5 1.6 %copy-done.6 = bf16[1,512,2048]{2,1,0:T(8,128)(2,1)S(1)} copy-done((bf16[1,512,2048]{2,1,0:T(8,128)(2,1)S(1)}, bf16[1,512,2048]{2,1,0:T(8,128)(2,1)}, u32[]{:S(2)}) %copy-start.6) | copy-done | bytes 2097176
  72.1 34.8 %shard_map.268 = bf16[24,2048]{1,0:T(8,128)(2,1)S(1)} custom-call(bf16[32,4,2048]{2,1,0:T(4,128)(2,1)S(1)} %get-tuple-element.6.rows_ref, bf16[24,2048]{1,0:T(8,128)(2,1)S(1)} %get-tuple-element.7.normed_ref, f32[24,2048]{1,0:T(8,128)S(1)} %get-tuple-element.8.middle_ref, bf16[48,128]{1,0:T(8,128)(2,1)S(1)} %pad_maximum_fusion.coef_ref, ...), custom_call_target="tpu_custom_call" | custom-call | flops 1000000000 | bytes 60000000 | tf_op jit(solution)/shard_map/pallas_call | solution.py:435
  106.9 0.6 copy.48
  (28 shorter events, 0.2 us)
Async XLA Ops:
  0.6 1.2 %copy-start = (s32[768,4]{0,1:T(4,128)S(1)}, s32[768,4]{0,1:T(4,128)}, u32[]{:S(2)}) copy-start(s32[768,4]{0,1:T(4,128)} %param.42) | copy-start | bytes 36868
  0.6 49.1 %copy-start.21 = (bf16[256,256]{1,0:T(8,128)(2,1)S(1)}, bf16[256,256]{1,0:T(8,128)(2,1)}, u32[]{:S(2)}) copy-start(bf16[256,256]{1,0:T(8,128)(2,1)} %constant.33.clone.block_ref) | copy-start | bytes 393220
  0.7 49.1 %copy-start.19 = (bf16[2,192,768]{2,1,0:T(8,128)(2,1)S(1)}, bf16[2,192,768]{2,1,0:T(8,128)(2,1)}, u32[]{:S(2)}) copy-start(bf16[2,192,768]{2,1,0:T(8,128)(2,1)} %constant.30.clone.place_ref) | copy-start | bytes 1769476
  0.7 49.1 %copy-start.7 = (bf16[24,2048]{1,0:T(8,128)(2,1)S(1)}, bf16[24,2048]{1,0:T(8,128)(2,1)}, u32[]{:S(2)}) copy-start(bf16[24,2048]{1,0:T(8,128)(2,1)} %resid_ref.1) | copy-start | bytes 294916
  0.7 49.1 %copy-start.17 = (f32[1024]{0:T(1024)S(1)}, f32[1024]{0:T(1024)}, u32[]{:S(2)}) copy-start(f32[1024]{0:T(1024)} %param.38) | copy-start | bytes 12292
  0.7 49.1 %copy-start.16 = (f32[1024]{0:T(1024)S(1)}, f32[1024]{0:T(1024)}, u32[]{:S(2)}) copy-start(f32[1024]{0:T(1024)} %param.37) | copy-start | bytes 12292
  0.7 49.1 %copy-start.15 = (f32[1024]{0:T(1024)S(1)}, f32[1024]{0:T(1024)}, u32[]{:S(2)}) copy-start(f32[1024]{0:T(1024)} %param.36) | copy-start | bytes 12292
  0.7 49.1 %copy-start.14 = (f32[1024]{0:T(1024)S(1)}, f32[1024]{0:T(1024)}, u32[]{:S(2)}) copy-start(f32[1024]{0:T(1024)} %param.35) | copy-start | bytes 12292
  6.1 0.9 copy-start.8
  7.0 0.9 copy-start.9
  7.9 0.9 copy-start.10
  8.8 0.9 copy-start.11
  9.7 0.9 copy-start.12
  10.6 0.9 copy-start.13
  11.6 38.3 %copy-start.18 = (bf16[4096,128]{1,0:T(8,128)(2,1)S(1)}, bf16[4096,128]{1,0:T(8,128)(2,1)}, u32[]{:S(2)}) copy-start(bf16[4096,128]{1,0:T(8,128)(2,1)} %constant.32.clone.gather_ref) | copy-start | bytes 3145732
  11.6 38.3 %copy-start.20 = (bf16[64,4096]{1,0:T(8,128)(2,1)S(1)}, bf16[64,4096]{1,0:T(8,128)(2,1)}, u32[]{:S(2)}) copy-start(bf16[64,4096]{1,0:T(8,128)(2,1)} %constant.31.clone.spread_ref) | copy-start | bytes 1572868
  49.9 19.0 %copy-start.1 = (bf16[2048,512]{1,0:T(8,128)(2,1)S(1)}, bf16[2048,512]{1,0:T(8,128)(2,1)}, u32[]{:S(2)}) copy-start(bf16[2048,512]{1,0:T(8,128)(2,1)} %g0.1) | copy-start | bytes 6291460
  49.9 19.0 %copy-start.2 = (bf16[2048,512]{1,0:T(8,128)(2,1)S(1)}, bf16[2048,512]{1,0:T(8,128)(2,1)}, u32[]{:S(2)}) copy-start(bf16[2048,512]{1,0:T(8,128)(2,1)} %g1.1) | copy-start | bytes 6291460
  49.9 19.0 %copy-start.3 = (bf16[512,2048]{1,0:T(8,128)(2,1)S(1)}, bf16[512,2048]{1,0:T(8,128)(2,1)}, u32[]{:S(2)}) copy-start(bf16[512,2048]{1,0:T(8,128)(2,1)} %g2.1) | copy-start | bytes 6291460
  49.9 19.0 %copy-start.4 = (bf16[1,2048,512]{2,1,0:T(8,128)(2,1)S(1)}, bf16[1,2048,512]{2,1,0:T(8,128)(2,1)}, u32[]{:S(2)}) copy-start(bf16[1,2048,512]{2,1,0:T(8,128)(2,1)} %param.44) | copy-start | bytes 6291460
  68.9 1.6 %copy-start.5 = (bf16[1,2048,512]{2,1,0:T(8,128)(2,1)S(1)}, bf16[1,2048,512]{2,1,0:T(8,128)(2,1)}, u32[]{:S(2)}) copy-start(bf16[1,2048,512]{2,1,0:T(8,128)(2,1)} %param.45) | copy-start | bytes 6291460
  70.5 1.6 %copy-start.6 = (bf16[1,512,2048]{2,1,0:T(8,128)(2,1)S(1)}, bf16[1,512,2048]{2,1,0:T(8,128)(2,1)}, u32[]{:S(2)}) copy-start(bf16[1,512,2048]{2,1,0:T(8,128)(2,1)} %param.46) | copy-start | bytes 6291460

commit v4 on v3

--- a/solution.py
+++ b/solution.py
@@ -193,7 +193,7 @@
     depth, normed_ref, w0, w1, w2, w3, w4, w5, land_out,
     weight_ref, held, cols, land,
     z_send, z_recv, near_send, near_recv, half_send, half_recv, core_send, core_recv,
-    out_send, out_recv,
+    out_send, out_recv, load_sem,
 ):
     total = depth * PLANE
     tokens, model = normed_ref.shape
@@ -221,7 +221,11 @@
     def slot(of_plane, d):
         return held.at[of_plane, lax.rem(level + depth - d, depth)]
 
-    sent = []
+    loads = []
+    for i, w in enumerate((w0, w1, w2, w3, w4, w5)):
+        part = weight_ref.at[pl.ds(i * w.shape[0], w.shape[0])]
+        loads.append(pltpu.make_async_copy(w, part, load_sem.at[i]))
+        loads[-1].start()
     along_z = [None]
     for d in range(1, depth):
         there = lax.rem(me + PLANE * d, total)
@@ -237,9 +241,8 @@
         by_core[0].append(send(source, here, mate, core_send.at[0, d], core_recv.at[0, d]))
         if d == 0:
             held[plane, level] = normed_ref[...]
-            weight_ref[...] = jnp.concatenate(
-                [w[...] for w in (w0, w1, w2, w3, w4, w5)], axis=0
-            )
+            for load in loads:
+                load.wait()
 
     def compute(group):
         rows = held[group].astype(F32).reshape(depth * tokens, model).astype(BF16)
@@ -321,7 +324,8 @@
     return pl.pallas_call(
         functools.partial(project_kernel, depth),
         out_shape=jax.ShapeDtypeStruct((ep_size, tokens, width), BF16),
-        in_specs=[pl.BlockSpec(memory_space=pltpu.VMEM)] * 7,
+        in_specs=[pl.BlockSpec(memory_space=pltpu.VMEM)]
+        + [pl.BlockSpec(memory_space=pltpu.HBM)] * len(weights),
         out_specs=pl.BlockSpec(memory_space=pltpu.VMEM),
         scratch_shapes=[
             pltpu.VMEM((width, model), BF16),
@@ -332,10 +336,10 @@
             dma((2, depth)), dma((2, depth)),
             dma((2, depth)), dma((2, depth)),
             dma((4, depth)), dma((4, depth)),
-            dma((ep_size,)), dma((ep_size,)),
+            dma((ep_size,)), dma((ep_size,)), dma((len(weights),)),
         ],
         compiler_params=pltpu.CompilerParams(
-            has_side_effects=True, vmem_limit_bytes=40 * 1024 * 1024
+            has_side_effects=True, vmem_limit_bytes=60 * 1024 * 1024
         ),
         cost_estimate=pl.CostEstimate(flops=600_000_000, bytes_accessed=100_000_000, transcendentals=0),
     )(normed, *weights)
@@ -435,14 +439,14 @@
     return pl.pallas_call(
         functools.partial(experts_kernel, depth),
         out_shape=jax.ShapeDtypeStruct((tokens, model), BF16),
-        in_specs=[vmem] * 4 + [pl.BlockSpec(memory_space=pl.ANY)] * 6,
+        in_specs=[vmem] * 4 + [pl.BlockSpec(memory_space=pltpu.HBM)] * 6,
         out_specs=vmem,
         scratch_shapes=[pltpu.VMEM(w.shape, BF16) for w in weights]
         + [pltpu.VMEM(rows.shape, BF16)] * 3
         + [dma((6,))]
         + [dma((ep_size,))] * 4,
         compiler_params=pltpu.CompilerParams(
-            has_side_effects=True, vmem_limit_bytes=40 * 1024 * 1024
+            has_side_effects=True, vmem_limit_bytes=60 * 1024 * 1024
         ),
         cost_estimate=pl.CostEstimate(flops=1_000_000_000, bytes_accessed=60_000_000, transcendentals=0),
     )(rows, normed, middle, coef, *weights)

time: 108 us -> 108 us (level)
  local copies, waits for them, and re-layouts: 11.6 us -> 6.94 us
  Pallas kernels: 91.9 us -> 95.4 us
  other arithmetic: 3.06 us -> 4.37 us
    unnamed x45 -> x29, local copies, waits for them, and re-layouts: 9.32 us -> 4.7 us
    pallas_call x1, Pallas kernels: 38.2 us -> 39.9 us  [project(): pl.pallas_call(functools.partial(project_kernel, depth), out_shape=jax.Sh...]
    pallas_call x1, Pallas kernels: 34.8 us -> 36.5 us  [experts_step(): pl.pallas_call(functools.partial(experts_kernel, depth), out_shape=jax.Sh...]
where the time goes in v4:
time: 108 us
  Pallas kernels  95.4 us (88%)
  local copies, waits for them, and re-layouts  6.94 us (6%)
  other arithmetic  4.37 us (4%)
    pallas_call x1, Pallas kernels, project(): pl.pallas_call(functools.partial(project_kernel, depth), out_shape=jax.Sh...  39.9 us
    pallas_call x1, Pallas kernels, experts_step(): pl.pallas_call(functools.partial(experts_kernel, depth), out_shape=jax.Sh...  36.5 us
    pallas_call x1, Pallas kernels, mixer(): pl.pallas_call(mixer_kernel, grid=(tokens // group,), out_shape=(jax.Shap...  18.9 us
    unnamed x29, local copies, waits for them, and re-layouts  4.7 us
    convert_element_type x2, other arithmetic, rms_norm(): return (value_rows * scale * gain.astype(F32)).astype(BF16)  2.32 us

profile of v4, /device:TPU:0, one launch (start us, length us, event | category | flops | bytes accessed | tf_op | source)
XLA Modules:
  0.0 107.6 jit_solution(15750710014026602883)
XLA Ops:
  0.6 0.0 copy-start
  0.6 0.0 copy-start.12
  0.7 0.0 copy-start.9
  0.7 0.0 copy-start.11
  0.7 0.0 copy-start.10
  0.7 0.0 copy-start.2
  0.7 0.0 copy-start.8
  0.7 0.0 copy-start.7
  0.7 0.0 copy-start.6
  0.7 0.0 copy-start.5
  0.8 1.2 %fusion = f32[24]{0:T(128)S(1)} fusion(bf16[24,2048]{1,0:T(8,128)(2,1)} %resid_ref.1), kind=kLoop, calls=%fused_computation.2 | loop fusion | flops 147432 | bytes 98400 | tf_op jit(solution)/shard_map/reduce_sum | solution.py:22
  1.9 0.0 copy-done
  1.9 0.1 constant_dynamic-slice_fusion.1
  2.0 0.8 constant_dynamic-slice_fusion
  2.8 0.1 fusion.3
  2.9 0.1 copy.40
  3.0 0.1 select_reduce_fusion
  3.1 0.1 copy.45
  3.1 0.7 convert_element_type.33
  3.8 0.7 reshape.57.gain_ref
  4.5 0.1 copy.43
  4.7 0.1 copy.41
  4.8 0.1 eq.40
  4.9 0.1 copy.42
  5.0 0.1 copy.46
  5.1 0.6 pad_maximum_fusion.coef_ref
  5.7 0.1 copy.44.select_ref
  5.8 1.6 %fusion.2.normed_ref = bf16[24,2048]{1,0:T(8,128)(2,1)} fusion(bf16[24,2048]{1,0:T(8,128)(2,1)} %resid_ref.1, f32[2048]{0:T(1024)S(1)} %convert_element_type.33, f32[24]{0:T(128)S(1)} %add_rsqrt_fusion), kind=kLoop, calls=%fused_computation.4 | loop fusion | flops 196608 | bytes 204896 | tf_op jit(solution)/shard_map/convert_element_type | solution.py:23
  7.4 39.9 %shard_map.266.land_ref = bf16[32,24,192]{2,1,0:T(8,128)(2,1)} custom-call(bf16[24,2048]{1,0:T(8,128)(2,1)} %fusion.2.normed_ref, bf16[32,2048]{1,0:T(8,128)(2,1)} %bitcast.28, bf16[32,2048]{1,0:T(8,128)(2,1)} %bitcast.29, bf16[32,2048]{1,0:T(8,128)(2,1)} %bitcast.30, bf16[32,2048]{1,0:T(8,128)(2,1)} %bitcast.31, bf16[32,2048]{1,0:T(8,128)(2,1)} %bitcast.32, ...), custom_call_target="tpu_custom_call" | custom-call | flops 600000000 | bytes 100000000 | tf_op jit(solution)/shard_map/pallas_call | solution.py:324
  47.4 0.0 copy-done.12
  47.4 0.0 copy-done.9
  47.4 0.0 copy-done.11
  47.4 0.0 copy-done.10
  47.4 0.0 copy-done.2
  47.4 0.0 copy-done.8
  47.4 0.0 copy-done.7
  47.5 0.0 copy-done.6
  47.5 0.0 copy-done.5
  47.5 0.0 copy-start.13
  47.5 1.0 copy-done.13
  48.5 18.9 %shard_map.267 = (f32[24,16,4096]{2,1,0:T(8,128)}, f32[24,2048]{1,0:T(8,128)S(1)}, bf16[24,2048]{1,0:T(8,128)(2,1)S(1)}, bf16[32,4,2048]{2,1,0:T(4,128)(2,1)S(1)}) custom-call(bf16[32,24,192]{2,1,0:T(8,128)(2,1)S(1)} %copy-done.13, bf16[2,192,768]{2,1,0:T(8,128)(2,1)S(1)} %copy-done.10, bf16[64,4096]{1,0:T(8,128)(2,1)S(1)} %copy-done.11, ...), custom_call_target="tpu_custom_call" | custom-call | flops 4000000000 | bytes 20000000 | tf_op jit(solution)/shard_map/pallas_call | solution.py:168
  67.4 0.0 copy-start.1
  67.4 0.8 copy-done.1
  68.2 0.0 copy-start.3
  68.2 0.7 copy-done.3
  68.9 0.6 copy-done.4
  69.5 36.5 %shard_map.268 = bf16[24,2048]{1,0:T(8,128)(2,1)} custom-call(bf16[32,4,2048]{2,1,0:T(4,128)(2,1)} %copy-done.1, bf16[24,2048]{1,0:T(8,128)(2,1)} %copy-done.4, f32[24,2048]{1,0:T(8,128)} %copy-done.3, bf16[48,128]{1,0:T(8,128)(2,1)} %pad_maximum_fusion.coef_ref, bf16[2048,512]{1,0:T(8,128)(2,1)} %g0.1, bf16[2048,512]{1,0:T(8,128)(2,1)} %g1.1, ...), custom_call_target="tpu_custom_call" | custom-call | flops 1000000000 | bytes 60000000 | tf_op jit(solution)/shard_map/pallas_call | solution.py:439
  106.0 1.5 %copy.48 = bf16[24,2048]{1,0:T(8,128)(2,1)} copy(bf16[24,2048]{1,0:T(8,128)(2,1)} %shard_map.268) | data formatting | bytes 196608
  (12 shorter events, 0.2 us)
Async XLA Ops:
  0.6 1.3 %copy-start = (s32[768,4]{0,1:T(4,128)S(1)}, s32[768,4]{0,1:T(4,128)}, u32[]{:S(2)}) copy-start(s32[768,4]{0,1:T(4,128)} %param.42) | copy-start | bytes 36868
  0.6 46.7 %copy-start.12 = (bf16[256,256]{1,0:T(8,128)(2,1)S(1)}, bf16[256,256]{1,0:T(8,128)(2,1)}, u32[]{:S(2)}) copy-start(bf16[256,256]{1,0:T(8,128)(2,1)} %constant.33.clone.block_ref) | copy-start | bytes 393220
  0.7 46.7 %copy-start.9 = (bf16[4096,128]{1,0:T(8,128)(2,1)S(1)}, bf16[4096,128]{1,0:T(8,128)(2,1)}, u32[]{:S(2)}) copy-start(bf16[4096,128]{1,0:T(8,128)(2,1)} %constant.32.clone.gather_ref) | copy-start | bytes 3145732
  0.7 46.7 %copy-start.11 = (bf16[64,4096]{1,0:T(8,128)(2,1)S(1)}, bf16[64,4096]{1,0:T(8,128)(2,1)}, u32[]{:S(2)}) copy-start(bf16[64,4096]{1,0:T(8,128)(2,1)} %constant.31.clone.spread_ref) | copy-start | bytes 1572868
  0.7 46.7 %copy-start.10 = (bf16[2,192,768]{2,1,0:T(8,128)(2,1)S(1)}, bf16[2,192,768]{2,1,0:T(8,128)(2,1)}, u32[]{:S(2)}) copy-start(bf16[2,192,768]{2,1,0:T(8,128)(2,1)} %constant.30.clone.place_ref) | copy-start | bytes 1769476
  0.7 46.7 %copy-start.2 = (bf16[24,2048]{1,0:T(8,128)(2,1)S(1)}, bf16[24,2048]{1,0:T(8,128)(2,1)}, u32[]{:S(2)}) copy-start(bf16[24,2048]{1,0:T(8,128)(2,1)} %resid_ref.1) | copy-start | bytes 294916
  0.7 46.7 %copy-start.8 = (f32[1024]{0:T(1024)S(1)}, f32[1024]{0:T(1024)}, u32[]{:S(2)}) copy-start(f32[1024]{0:T(1024)} %param.38) | copy-start | bytes 12292
  0.7 46.7 %copy-start.7 = (f32[1024]{0:T(1024)S(1)}, f32[1024]{0:T(1024)}, u32[]{:S(2)}) copy-start(f32[1024]{0:T(1024)} %param.37) | copy-start | bytes 12292
  0.7 46.7 %copy-start.6 = (f32[1024]{0:T(1024)S(1)}, f32[1024]{0:T(1024)}, u32[]{:S(2)}) copy-start(f32[1024]{0:T(1024)} %param.36) | copy-start | bytes 12292
  0.7 46.7 %copy-start.5 = (f32[1024]{0:T(1024)S(1)}, f32[1024]{0:T(1024)}, u32[]{:S(2)}) copy-start(f32[1024]{0:T(1024)} %param.35) | copy-start | bytes 12292
  47.5 1.0 copy-start.13
  67.4 0.8 copy-start.1
  68.2 0.7 copy-start.3
  68.9 0.6 copy-start.4
